TPU v7x, 32 devices: a whole 2x2x4 slice. The times are simulated.
32 devices in a mesh: kv: 8 (over z, y), tp: 4 (over x, core).
Axes of the slice: x: 2, y: 2, z: 4, core: 2. Of those that a mesh axis runs over, the one named last changes fastest.
Arguments:
- activations: bfloat16 [64, 4096], P(None, ('kv', 'tp')), may hold values from -60 to 60
- mixer_gain: bfloat16 [4096], P(('kv', 'tp')), may hold values from 0.099609375 to 1.8984375
- channel_gain: bfloat16 [4096], P(('kv', 'tp')), may hold values from 0.099609375 to 1.8984375
- query_weight: bfloat16 [4096, 4096], P('kv', 'tp'), may hold values from -0.09375 to 0.09375
- key_weight: bfloat16 [4096, 4096], P('kv', 'tp'), may hold values from -0.09375 to 0.09375
- value_weight: bfloat16 [4096, 8192], P('kv', 'tp'), may hold values from -0.09375 to 0.09375
- gate_weight: bfloat16 [4096, 8192], P('kv', 'tp'), may hold values from -0.09375 to 0.09375
- output_weight: bfloat16 [8192, 4096], P('tp', 'kv'), may hold values from -0.1875 to 0.1875
- up_weight: bfloat16 [4096, 16384], P('kv', 'tp'), may hold values from -0.09375 to 0.09375
- down_weight: bfloat16 [16384, 4096], P('tp', 'kv'), may hold values from -0.046875 to 0.046875
- state_in: float32 [64, 16, 256, 512], P('kv', 'tp'), may hold values from -0.5 to 0.5
Outputs:
- activations_out: bfloat16 [64, 4096], P(None, ('kv', 'tp'))
- state_out: float32 [64, 16, 256, 512], P('kv', 'tp')
All inputs are finite; a program needn't handle non-finite values.
Results may differ from a plain program's by a relative error of at most 0.022.
Values may be sent and summed in bfloat16 or wider, within the bound.
A program may use at most 128 MiB of HBM per device.

v0:
```python
import functools

import jax
import jax.numpy as jnp
from jax import lax
from jax.experimental import pallas as pl
from jax.experimental.pallas import tpu as pltpu
from jax.sharding import PartitionSpec as P

HEADS = 16
EPS = 1e-06
MESH = pl.DeviceIdType.MESH
F32 = jnp.float32
BF16 = jnp.bfloat16
DMA = pltpu.SemaphoreType.DMA
PAIR = 2
LAG = 2


def head_decays(count):
    index = jnp.arange(count, dtype=jnp.float32)
    return 1.0 - 2.0 ** (-1.0 - 6.0 * index / (count - 1))


def put(src, dst, send_sem, recv_sem, where):
    copy = pltpu.make_async_remote_copy(
        src_ref=src,
        dst_ref=dst,
        send_sem=send_sem,
        recv_sem=recv_sem,
        device_id=where,
        device_id_type=MESH,
    )
    copy.start()
    return copy


def greet(kv, tp, n_kv, n_tp):
    barrier = pltpu.get_barrier_semaphore()
    for d in range(1, n_tp):
        pl.semaphore_signal(
            barrier, inc=1, device_id={"tp": lax.rem(tp + d, n_tp)}, device_id_type=MESH
        )
    for d in range(1, n_kv):
        pl.semaphore_signal(
            barrier, inc=1, device_id={"kv": lax.rem(kv + d, n_kv)}, device_id_type=MESH
        )
    pl.semaphore_wait(barrier, n_tp + n_kv - 2)


def tp_gather(buf, tp, n_tp, sems):
    return [
        put(
            buf.at[tp],
            buf.at[tp],
            sems.at[0, d - 1],
            sems.at[1, d - 1],
            {"tp": lax.rem(tp + d, n_tp)},
        )
        for d in range(1, n_tp)
    ]


def tp_scatter(src, dst, tp, n_tp, sems):
    copies = []
    for d in range(1, n_tp):
        peer = lax.rem(tp + d, n_tp)
        copies.append(
            put(src.at[peer], dst.at[d - 1], sems.at[0, d - 1], sems.at[1, d - 1], {"tp": peer})
        )
    return copies


def kv_scatter_small(src, dst, kv, n_kv, sems):
    copies = []
    for d in range(1, n_kv):
        peer = lax.rem(kv + d, n_kv)
        copies.append(
            put(src.at[peer], dst.at[d - 1], sems.at[0, d - 1], sems.at[1, d - 1], {"kv": peer})
        )
    return copies


def own_square_total(squares, sq_src, sq_dst, kv, n_kv, rows, sems):
    for g in range(n_kv):
        sq_src[g] = jnp.broadcast_to(squares[g * rows : (g + 1) * rows], sq_src.shape[1:])
    copies = kv_scatter_small(sq_src, sq_dst, kv, n_kv, sems)

    def finish():
        total = sq_src[kv]
        for d, copy in enumerate(copies):
            copy.wait_recv()
            total = total + sq_dst[d]
        return total[:, :1]

    return copies, finish


class PairScatter:
    def __init__(self, kv, n_kv, rows, part, got, summed, got2, sem_a, sem_b):
        self.n_z = n_kv // PAIR
        self.z, self.y = lax.div(kv, PAIR), lax.rem(kv, PAIR)
        self.rows = rows
        self.part, self.got, self.summed, self.got2 = part, got, summed, got2
        self.sem_a, self.sem_b = sem_a, sem_b
        self.first, self.second = {}, {}

    def start(self, p, value):
        rows = self.rows
        for z in range(self.n_z):
            for y in range(PAIR):
                at = (z * PAIR + y) * rows
                self.part[p, y, z] = value[at : at + rows].astype(BF16)
        other = 1 - self.y
        self.first[p] = put(
            self.part.at[p, other],
            self.got.at[p],
            self.sem_a.at[0, p],
            self.sem_a.at[1, p],
            {"kv": self.z * PAIR + other},
        )

    def middle(self, p):
        self.first[p].wait_recv()
        self.summed[p] = (self.part[p, self.y].astype(F32) + self.got[p].astype(F32)).astype(BF16)
        copies = []
        for d in range(1, self.n_z):
            peer = lax.rem(self.z + d, self.n_z)
            copies.append(
                put(
                    self.summed.at[p, peer],
                    self.got2.at[p, d - 1],
                    self.sem_b.at[0, p, d - 1],
                    self.sem_b.at[1, p, d - 1],
                    {"kv": peer * PAIR + self.y},
                )
            )
        self.second[p] = copies

    def finish(self, p):
        total = self.summed[p, self.z].astype(F32)
        for d, copy in enumerate(self.second[p]):
            copy.wait_recv()
            total = total + self.got2[p, d].astype(F32)
        return total

    def drain(self):
        for p in self.first:
            self.first[p].wait_send()
            for copy in self.second[p]:
                copy.wait_send()


class PairGather:
    def __init__(self, kv, n_kv, buf, sem_z, sem_y):
        self.n_z = n_kv // PAIR
        self.z, self.y = lax.div(kv, PAIR), lax.rem(kv, PAIR)
        self.buf, self.sem_z, self.sem_y = buf, sem_z, sem_y
        self.along, self.across = {}, {}

    def forward(self, p, d):
        z = lax.rem(self.z - d + self.n_z, self.n_z)
        self.across[p].append(
            put(
                self.buf.at[p, z, self.y],
                self.buf.at[p, z, self.y],
                self.sem_y.at[0, p, d],
                self.sem_y.at[1, p, d],
                {"kv": self.z * PAIR + 1 - self.y},
            )
        )

    def start(self, p):
        own = self.buf.at[p, self.z, self.y]
        self.along[p], self.across[p] = [], []
        for d in range(1, self.n_z):
            peer = lax.rem(self.z + d, self.n_z)
            self.along[p].append(
                put(
                    own,
                    own,
                    self.sem_z.at[0, p, d - 1],
                    self.sem_z.at[1, p, d - 1],
                    {"kv": peer * PAIR + self.y},
                )
            )
        self.forward(p, 0)

    def relay(self, p):
        for d, copy in enumerate(self.along[p]):
            copy.wait_recv()
            self.forward(p, d + 1)

    def finish(self, p):
        for copy in self.across[p]:
            copy.wait_recv()
        blocks = [
            self.buf[p, z, y].astype(F32) for z in range(self.n_z) for y in range(PAIR)
        ]
        return jnp.concatenate(blocks, axis=0).astype(BF16)

    def drain(self):
        for p in self.along:
            for copy in self.along[p] + self.across[p]:
                copy.wait_send()


def project_kernel(
    sizes,
    x_ref,
    gain_ref,
    *refs,
):
    n_kv, n_tp, rows, width, counts, dim = sizes
    weights, refs = refs[:4], refs[4:]
    old, outs, held, refs = refs[0], refs[1:5], refs[5], refs[6:]
    (xs, gains, w, part, got, summed, got2, sq_src, sq_dst) = refs[:9]
    (w_sem, x_sem, g_sem, sq_sem, sem_a, sem_b, s_sem) = refs[9:]
    kv, tp = lax.axis_index("kv"), lax.axis_index("tp")
    pieces = [(i, j) for i, count in enumerate(counts) for j in range(count)]
    loads = []
    for p, (i, j) in enumerate(pieces):
        load = pltpu.make_async_copy(
            weights[i].at[:, pl.ds(j * width, width)], w.at[p], w_sem.at[p]
        )
        load.start()
        loads.append(load)
    state_load = pltpu.make_async_copy(old, held, s_sem)
    state_load.start()
    xs[tp] = x_ref[...]
    gains[tp] = jnp.broadcast_to(gain_ref[...].astype(F32), gains.shape[1:])
    greet(kv, tp, n_kv, n_tp)
    x_copies = tp_gather(xs, tp, n_tp, x_sem)
    g_copies = tp_gather(gains, tp, n_tp, g_sem)
    for copy in x_copies + g_copies:
        copy.wait_recv()
    stream = [xs[t].astype(F32) for t in range(n_tp)]
    normed = jnp.concatenate(
        [(stream[t] * gains[t][:1]).astype(BF16) for t in range(n_tp)], axis=1
    )
    squares = sum(jnp.sum(s * s, axis=1, keepdims=True) for s in stream)
    sq_copies, sq_total = own_square_total(squares, sq_src, sq_dst, kv, n_kv, rows, sq_sem)
    scatter = PairScatter(kv, n_kv, rows, part, got, summed, got2, sem_a, sem_b)
    for p in range(len(pieces)):
        loads[p].wait()
        scatter.start(p, jnp.dot(normed, w[p], preferred_element_type=F32))
        if p >= LAG:
            scatter.middle(p - LAG)
    for p in range(max(len(pieces) - LAG, 0), len(pieces)):
        scatter.middle(p)
    scale = lax.rsqrt(sq_total() / dim + EPS)
    for p, (i, j) in enumerate(pieces):
        outs[i][:, j * width : (j + 1) * width] = scatter.finish(p) * scale
    state_load.wait()
    scatter.drain()
    for copy in x_copies + g_copies + sq_copies:
        copy.wait_send()


def retain_kernel(
    heads, dk, dv, q_ref, k_ref, v_ref, g_ref, rate_ref, old_ref, out_ref, mix_ref, new_ref, sem
):
    step = min(dk, 64)
    seqs = q_ref.shape[0]

    def write(s):
        return pltpu.make_async_copy(new_ref.at[s], out_ref.at[s], sem.at[s])

    def one(s, carry):
        q_row = q_ref[pl.ds(s, 1), :]
        k_row = k_ref[pl.ds(s, 1), :] * dk ** (-0.5)
        lines = [q_row[:, h * dk : (h + 1) * dk] for h in range(heads)]
        lines += [k_row[:, h * dk : (h + 1) * dk] for h in range(heads)]
        if len(lines) % 8:
            lines.append(jnp.zeros((8 - len(lines) % 8, dk), F32))
        columns = jnp.concatenate(lines, axis=0).T
        for h in range(heads):
            span = slice(h * dv, (h + 1) * dv)
            value = v_ref[pl.ds(s, 1), span]
            total = jnp.zeros((8, dv), F32)
            for r in range(0, dk, step):
                query = columns[r : r + step, h : h + 1]
                key = columns[r : r + step, heads + h : heads + h + 1]
                new = rate_ref[h] * old_ref[s, h, r : r + step] + key * value
                new_ref[s, h, r : r + step] = new
                total = total + jnp.sum((query * new).reshape(step // 8, 8, dv), axis=0)
            out = jnp.sum(total, axis=0, keepdims=True)
            out = out * lax.rsqrt(jnp.mean(out * out, axis=1, keepdims=True) + EPS)
            mix_ref[pl.ds(s, 1), span] = jax.nn.silu(g_ref[pl.ds(s, 1), span]) * out
        write(s).start()
        return carry

    lax.fori_loop(0, seqs, one, 0, unroll=4)
    for s in range(seqs):
        write(s).wait()


def mix_kernel(sizes, mix_ref, x_ref, gain_ref, ow_hbm, up_hbm, down_hbm, out_ref, *refs):
    n_kv, n_tp, rows, width, count, dim = sizes
    (ow, up, down, mixes, gains, ends, got_ends, mids, part, got, summed, got2) = refs[:12]
    (sq_src, sq_dst, hid, w_sem, g_sem, mz_sem, my_sem, e_sem, m_sem, sq_sem) = refs[12:22]
    (sem_a, sem_b, hz_sem, hy_sem, f_sem) = refs[22:]
    kv, tp = lax.axis_index("kv"), lax.axis_index("tp")
    z, y = lax.div(kv, PAIR), lax.rem(kv, PAIR)
    block = x_ref.shape[1]
    ow_load = pltpu.make_async_copy(ow_hbm, ow, w_sem.at[0])
    ow_load.start()
    ups, downs = [], []
    for p in range(count):
        load = pltpu.make_async_copy(
            up_hbm.at[:, pl.ds(p * width, width)], up.at[p], w_sem.at[1 + p]
        )
        load.start()
        ups.append(load)
    for p in range(count):
        load = pltpu.make_async_copy(
            down_hbm.at[pl.ds(p * width, width), :], down.at[p], w_sem.at[1 + count + p]
        )
        load.start()
        downs.append(load)
    mixes[0, z, y] = mix_ref[...].astype(BF16)
    gains[tp] = jnp.broadcast_to(gain_ref[...].astype(F32), gains.shape[1:])
    greet(kv, tp, n_kv, n_tp)
    mix_gather = PairGather(kv, n_kv, mixes, mz_sem, my_sem)
    mix_gather.start(0)
    g_copies = tp_gather(gains, tp, n_tp, g_sem)
    mix_gather.relay(0)
    mixed = mix_gather.finish(0)
    ow_load.wait()

    def tp_sum(terms, at, sems):
        for t in range(n_tp):
            ends[at, t] = terms[:, t * block : (t + 1) * block].astype(BF16)
        copies = tp_scatter(ends.at[at], got_ends.at[at], tp, n_tp, sems)
        total = ends[at, tp].astype(F32)
        for d, copy in enumerate(copies):
            copy.wait_recv()
            total = total + got_ends[at, d].astype(F32)
        return copies, total

    e_copies, attention = tp_sum(jnp.dot(mixed, ow[...], preferred_element_type=F32), 0, e_sem)
    mids[tp] = (x_ref[...].astype(F32) + attention).astype(BF16)
    m_copies = tp_gather(mids, tp, n_tp, m_sem)
    for copy in g_copies + m_copies:
        copy.wait_recv()
    stream = [mids[t].astype(F32) for t in range(n_tp)]
    normed = jnp.concatenate(
        [(stream[t] * gains[t][:1]).astype(BF16) for t in range(n_tp)], axis=1
    )
    squares = sum(jnp.sum(s * s, axis=1, keepdims=True) for s in stream)
    sq_copies, sq_total = own_square_total(squares, sq_src, sq_dst, kv, n_kv, rows, sq_sem)
    scatter = PairScatter(kv, n_kv, rows, part, got, summed, got2, sem_a, sem_b)
    gather = PairGather(kv, n_kv, hid, hz_sem, hy_sem)
    for p in range(count):
        ups[p].wait()
        scatter.start(p, jnp.dot(normed, up[p], preferred_element_type=F32))
        if p >= LAG:
            scatter.middle(p - LAG)
    for p in range(max(count - LAG, 0), count):
        scatter.middle(p)
    scale = lax.rsqrt(sq_total() / dim + EPS)
    for p in range(count):
        lifted = scatter.finish(p) * scale
        hid[p, z, y] = jnp.square(jnp.maximum(lifted, 0.0)).astype(BF16)
        gather.start(p)
        if p >= 1:
            gather.relay(p - 1)
    gather.relay(count - 1)
    terms = None
    for p in range(count):
        hidden = gather.finish(p)
        downs[p].wait()
        term = jnp.dot(hidden, down[p], preferred_element_type=F32)
        terms = term if terms is None else terms + term
    f_copies, lowered = tp_sum(terms, 1, f_sem)
    out_ref[...] = (mids[tp].astype(F32) + lowered).astype(BF16)
    mix_gather.drain()
    gather.drain()
    scatter.drain()
    for copy in g_copies + e_copies + m_copies + sq_copies + f_copies:
        copy.wait_send()


def in_hbm(a):
    return pltpu.with_memory_space_constraint(a, pltpu.HBM)


VM = pl.BlockSpec(memory_space=pltpu.VMEM)
ANY = pl.BlockSpec(memory_space=pltpu.HBM)


def scatter_scratch(count, n_kv, rows, width):
    n_z = n_kv // PAIR
    return [
        pltpu.VMEM((count, PAIR, n_z, rows, width), BF16),
        pltpu.VMEM((count, n_z, rows, width), BF16),
        pltpu.VMEM((count, n_z, rows, width), BF16),
        pltpu.VMEM((count, n_z - 1, rows, width), BF16),
    ]


def fused_device(n_kv, n_tp, x, mg, cg, qw, kw, vw, gw, ow, uw, dw, state):
    seqs, heads, dk, dv = state.shape
    batch, block = x.shape
    dim = block * n_kv * n_tp
    n_z = n_kv // PAIR
    depth, width = qw.shape
    counts = tuple(m.shape[1] // width for m in (qw, kw, vw, gw))
    pieces = sum(counts)
    params = functools.partial(pltpu.CompilerParams, has_side_effects=True)
    query, key, value, gate, held = pl.pallas_call(
        functools.partial(project_kernel, (n_kv, n_tp, seqs, width, counts, dim)),
        out_shape=[jax.ShapeDtypeStruct((seqs, m.shape[1]), F32) for m in (qw, kw, vw, gw)]
        + [pltpu.VMEM(state.shape, F32)],
        in_specs=[VM, VM] + [ANY] * 5,
        out_specs=[VM] * 4 + [pl.BlockSpec(memory_space=pltpu.VMEM)],
        scratch_shapes=[
            pltpu.VMEM((n_tp, batch, block), BF16),
            pltpu.VMEM((n_tp, 8, block), F32),
            pltpu.VMEM((pieces, depth, width), BF16),
            *scatter_scratch(pieces, n_kv, seqs, width),
            pltpu.VMEM((n_kv, seqs, 128), F32),
            pltpu.VMEM((n_kv - 1, seqs, 128), F32),
            DMA((pieces,)),
            DMA((2, n_tp - 1)),
            DMA((2, n_tp - 1)),
            DMA((2, n_kv - 1)),
            DMA((2, pieces)),
            DMA((2, pieces, n_z - 1)),
            DMA,
        ],
        compiler_params=params(collective_id=0, vmem_limit_bytes=13 * 2**20),
        cost_estimate=pl.CostEstimate(
            flops=2 * batch * depth * width * pieces,
            bytes_accessed=2 * depth * width * pieces * 8,
            transcendentals=0,
        ),
        name="project",
    )(x, mg.reshape(1, block), *[in_hbm(a) for a in (qw, kw, vw, gw, state)])
    rates = lax.dynamic_slice_in_dim(
        head_decays(HEADS), lax.axis_index("tp") * heads, heads, 0
    )
    new_state, mixed = pl.pallas_call(
        functools.partial(retain_kernel, heads, dk, dv),
        out_shape=[
            pltpu.HBM(state.shape, F32),
            jax.ShapeDtypeStruct((seqs, heads * dv), F32),
        ],
        in_specs=[VM] * 4 + [pl.BlockSpec(memory_space=pltpu.SMEM), VM],
        out_specs=[
            ANY,
            VM,
        ],
        scratch_shapes=[pltpu.VMEM(state.shape, F32), DMA((seqs,))],
        compiler_params=pltpu.CompilerParams(vmem_limit_bytes=18 * 2**20),
        cost_estimate=pl.CostEstimate(
            flops=6 * state.size, bytes_accessed=8 * state.size, transcendentals=0
        ),
        name="retain",
    )(query, key, value, gate, rates, held)
    width = min(1024, uw.shape[1])
    count = uw.shape[1] // width
    out = pl.pallas_call(
        functools.partial(mix_kernel, (n_kv, n_tp, seqs, width, count, dim)),
        out_shape=jax.ShapeDtypeStruct((batch, block), BF16),
        in_specs=[VM, VM, VM, ANY, ANY, ANY],
        out_specs=VM,
        scratch_shapes=[
            pltpu.VMEM(ow.shape, BF16),
            pltpu.VMEM((count, depth, width), BF16),
            pltpu.VMEM((count, width, dw.shape[1]), BF16),
            pltpu.VMEM((1, n_z, PAIR, seqs, heads * dv), BF16),
            pltpu.VMEM((n_tp, 8, block), F32),
            pltpu.VMEM((2, n_tp, batch, block), BF16),
            pltpu.VMEM((2, n_tp - 1, batch, block), BF16),
            pltpu.VMEM((n_tp, batch, block), BF16),
            *scatter_scratch(count, n_kv, seqs, width),
            pltpu.VMEM((n_kv, seqs, 128), F32),
            pltpu.VMEM((n_kv - 1, seqs, 128), F32),
            pltpu.VMEM((count, n_z, PAIR, seqs, width), BF16),
            DMA((1 + 2 * count,)),
            DMA((2, n_tp - 1)),
            DMA((2, 1, n_z - 1)),
            DMA((2, 1, n_z)),
            DMA((2, n_tp - 1)),
            DMA((2, n_tp - 1)),
            DMA((2, n_kv - 1)),
            DMA((2, count)),
            DMA((2, count, n_z - 1)),
            DMA((2, count, n_z - 1)),
            DMA((2, count, n_z)),
            DMA((2, n_tp - 1)),
        ],
        compiler_params=params(collective_id=1, vmem_limit_bytes=18 * 2**20),
        cost_estimate=pl.CostEstimate(
            flops=4 * batch * depth * uw.shape[1],
            bytes_accessed=4 * depth * uw.shape[1] * 16,
            transcendentals=0,
        ),
        name="mix",
    )(mixed, x, cg.reshape(1, block), *[in_hbm(a) for a in (ow, uw, dw)])
    return out, new_state


def solution(mesh):
    return jax.shard_map(
        functools.partial(fused_device, mesh.shape["kv"], mesh.shape["tp"]),
        mesh=mesh,
        in_specs=(
            P(None, ("kv", "tp")),
            P(("kv", "tp")),
            P(("kv", "tp")),
            P("kv", "tp"),
            P("kv", "tp"),
            P("kv", "tp"),
            P("kv", "tp"),
            P("tp", "kv"),
            P("kv", "tp"),
            P("tp", "kv"),
            P("kv", "tp", None, None),
        ),
        out_specs=(P(None, ("kv", "tp")), P("kv", "tp", None, None)),
        check_vma=False,
    )
```

profile of v0, /device:TPU:0, one launch (start us, length us, event | category | flops | bytes accessed | tf_op | source)
XLA Modules:
  0.0 77.2 jit_solution(5335698004780987562)
XLA Ops:
  0.6 0.1 dynamic_slice.3.rate_ref
  0.7 0.0 copy-start
  0.7 0.7 copy-done
  1.4 0.0 copy-start.2
  1.4 0.7 copy-done.2
  2.1 23.8 %project.1 = (f32[8,1024]{1,0:T(8,128)S(1)}, f32[8,1024]{1,0:T(8,128)S(1)}, f32[8,2048]{1,0:T(8,128)S(1)}, f32[8,2048]{1,0:T(8,128)S(1)}, f32[8,4,256,512]{3,2,1,0:T(8,128)S(1)}) custom-call(bf16[64,128]{1,0:T(8,128)(2,1)S(1)} %copy-done, bf16[1,128]{1,0:T(2,128)(2,1)S(1)} %bitcast.2, bf16[512,1024]{1,0:T(8,128)(2,1)} %refs_0_.1, bf16[512,1024]{1,0:T(8,128)(2,1)} %refs_1_.1, ...), custom_call_target="tpu_custom_call" | custom-call | flops 402653184 | bytes 50331648 | tf_op jit(solution)/shard_map/project/pallas_call | solution.py:411
  25.9 0.0 copy-start.1
  25.9 0.0 copy-start.3
  25.9 7.5 %retain.1 = (f32[8,4,256,512]{3,2,1,0:T(8,128)}, f32[8,2048]{1,0:T(8,128)S(1)}) custom-call(f32[8,1024]{1,0:T(8,128)S(1)} %get-tuple-element.9.q_ref, f32[8,1024]{1,0:T(8,128)S(1)} %get-tuple-element.10.k_ref, f32[8,2048]{1,0:T(8,128)S(1)} %get-tuple-element.11.v_ref, f32[8,2048]{1,0:T(8,128)S(1)} %get-tuple-element.12.g_ref, f32[4]{0:T(128)S(1)} %dynamic_slice.3.rate_ref, ...), custom_call_target="tpu_custom_call" | custom-call | flops 25165824 | bytes 33554432 | tf_op jit(solution)/shard_map/retain/pallas_call | solution.py:443
  33.5 0.0 copy-done.1
  33.5 0.0 copy-done.3
  33.5 43.1 %mix.1 = bf16[64,128]{1,0:T(8,128)(2,1)S(1)} custom-call(f32[8,2048]{1,0:T(8,128)S(1)} %get-tuple-element.14.mix_ref, bf16[64,128]{1,0:T(8,128)(2,1)S(1)} %copy-done.1, bf16[1,128]{1,0:T(2,128)(2,1)S(1)} %bitcast.3, bf16[2048,512]{1,0:T(8,128)(2,1)} %ow_hbm.1, bf16[512,4096]{1,0:T(8,128)(2,1)} %up_hbm.1, bf16[4096,512]{1,0:T(8,128)(2,1)} %down_hbm.1), custom_call_target="tpu_custom_call" | custom-call | flops 536870912 | bytes 134217728 | tf_op jit(solution)/shard_map/mix/pallas_call | solution.py:463
  76.6 0.6 copy.14
  (1 shorter events, 0.0 us)
Async XLA Ops:
  0.7 0.7 copy-start
  1.4 0.7 copy-start.2
  25.9 7.6 %copy-start.1 = (bf16[64,128]{1,0:T(8,128)(2,1)S(1)}, bf16[64,128]{1,0:T(8,128)(2,1)}, u32[]{:S(2)}) copy-start(bf16[64,128]{1,0:T(8,128)(2,1)} %x_ref.3) | copy-start | bytes 49156
  25.9 7.6 %copy-start.3 = (bf16[128]{0:T(256)(128)(2,1)S(1)}, bf16[128]{0:T(256)(128)(2,1)}, u32[]{:S(2)}) copy-start(bf16[128]{0:T(256)(128)(2,1)} %param.13) | copy-start | bytes 772
where the time goes:
time: 77.5 us; the launch traced here: 77.2 us
  Pallas kernels  74.4 us (96%)
  local copies, waits for them, and re-layouts  2.07 us (3%)
    pallas_call x1, Pallas kernels, fused_device(): pl.pallas_call(functools.partial(mix_kernel, (n_kv, n_tp, seqs, width, co...  43.1 us
    pallas_call x1, Pallas kernels, fused_device(): pl.pallas_call(functools.partial(project_kernel, (n_kv, n_tp, seqs, width...  23.8 us
    pallas_call x1, Pallas kernels, fused_device(): pl.pallas_call(functools.partial(retain_kernel, heads, dk, dv), out_shape...  7.52 us
    unnamed x9, local copies, waits for them, and re-layouts  1.99 us

commit v1 on v0

v1 whole, which is shorter than its diff:
```python
import functools

import jax
import jax.numpy as jnp
from jax import lax
from jax.experimental import pallas as pl
from jax.experimental.pallas import tpu as pltpu
from jax.sharding import PartitionSpec as P

HEADS = 16
EPS = 1e-06
MESH = pl.DeviceIdType.MESH
F32 = jnp.float32
BF16 = jnp.bfloat16
DMA = pltpu.SemaphoreType.DMA
PAIR = 2
CORES = 2
GAIN_ROWS = 16
WIDTH = 512
LAG_A, LAG_B = 5, 5
LAG_1, LAG_2, LAG_3, LAG_4 = 4, 4, 4, 3


def head_decays(count):
    index = jnp.arange(count, dtype=jnp.float32)
    return 1.0 - 2.0 ** (-1.0 - 6.0 * index / (count - 1))


def put(src, dst, send_sem, recv_sem, where):
    copy = pltpu.make_async_remote_copy(
        src_ref=src,
        dst_ref=dst,
        send_sem=send_sem,
        recv_sem=recv_sem,
        device_id=where,
        device_id_type=MESH,
    )
    copy.start()
    return copy


def tp_gather(buf, tp, n_tp, sems):
    return [
        put(
            buf.at[tp],
            buf.at[tp],
            sems.at[0, d - 1],
            sems.at[1, d - 1],
            {"tp": lax.rem(tp + d, n_tp)},
        )
        for d in range(1, n_tp)
    ]


def tp_scatter(src, dst, tp, n_tp, sems):
    copies = []
    for d in range(1, n_tp):
        peer = lax.rem(tp + d, n_tp)
        copies.append(
            put(src.at[peer], dst.at[d - 1], sems.at[0, d - 1], sems.at[1, d - 1], {"tp": peer})
        )
    return copies


def kv_scatter_small(src, dst, kv, n_kv, sems):
    copies = []
    for d in range(1, n_kv):
        peer = lax.rem(kv + d, n_kv)
        copies.append(
            put(src.at[peer], dst.at[d - 1], sems.at[0, d - 1], sems.at[1, d - 1], {"kv": peer})
        )
    return copies


def own_square_total(squares, sq_src, sq_dst, kv, n_kv, rows, sems):
    for g in range(n_kv):
        sq_src[g] = jnp.broadcast_to(squares[g * rows : (g + 1) * rows], sq_src.shape[1:])
    copies = kv_scatter_small(sq_src, sq_dst, kv, n_kv, sems)

    def finish():
        total = sq_src[kv]
        for d, copy in enumerate(copies):
            copy.wait_recv()
            total = total + sq_dst[d]
        return total[:, :1]

    return copies, finish


class PairScatter:
    def __init__(self, kv, n_kv, rows, part, got, summed, got2, sem_a, sem_b):
        self.n_z = n_kv // PAIR
        self.z, self.y = lax.div(kv, PAIR), lax.rem(kv, PAIR)
        self.rows = rows
        self.part, self.got, self.summed, self.got2 = part, got, summed, got2
        self.sem_a, self.sem_b = sem_a, sem_b
        self.first, self.second = {}, {}

    def start(self, p, value):
        rows = self.rows
        for z in range(self.n_z):
            for y in range(PAIR):
                at = (z * PAIR + y) * rows
                self.part[p, y, z] = value[at : at + rows].astype(BF16)
        other = 1 - self.y
        self.first[p] = put(
            self.part.at[p, other],
            self.got.at[p],
            self.sem_a.at[0, p],
            self.sem_a.at[1, p],
            {"kv": self.z * PAIR + other},
        )

    def middle(self, p):
        self.first[p].wait_recv()
        self.summed[p] = (self.part[p, self.y].astype(F32) + self.got[p].astype(F32)).astype(BF16)
        copies = []
        for d in range(1, self.n_z):
            peer = lax.rem(self.z + d, self.n_z)
            copies.append(
                put(
                    self.summed.at[p, peer],
                    self.got2.at[p, d - 1],
                    self.sem_b.at[0, p, d - 1],
                    self.sem_b.at[1, p, d - 1],
                    {"kv": peer * PAIR + self.y},
                )
            )
        self.second[p] = copies

    def finish(self, p):
        total = self.summed[p, self.z].astype(F32)
        for d, copy in enumerate(self.second[p]):
            copy.wait_recv()
            total = total + self.got2[p, d].astype(F32)
        return total

    def drain(self):
        for p in self.first:
            self.first[p].wait_send()
            for copy in self.second[p]:
                copy.wait_send()


class PairGather:
    def __init__(self, kv, n_kv, buf, sem_z, sem_y):
        self.n_z = n_kv // PAIR
        self.z, self.y = lax.div(kv, PAIR), lax.rem(kv, PAIR)
        self.buf, self.sem_z, self.sem_y = buf, sem_z, sem_y
        self.along, self.across = {}, {}

    def forward(self, p, d):
        z = lax.rem(self.z - d + self.n_z, self.n_z)
        self.across[p].append(
            put(
                self.buf.at[p, z, self.y],
                self.buf.at[p, z, self.y],
                self.sem_y.at[0, p, d],
                self.sem_y.at[1, p, d],
                {"kv": self.z * PAIR + 1 - self.y},
            )
        )

    def start(self, p):
        own = self.buf.at[p, self.z, self.y]
        self.along[p], self.across[p] = [], []
        for d in range(1, self.n_z):
            peer = lax.rem(self.z + d, self.n_z)
            self.along[p].append(
                put(
                    own,
                    own,
                    self.sem_z.at[0, p, d - 1],
                    self.sem_z.at[1, p, d - 1],
                    {"kv": peer * PAIR + self.y},
                )
            )
        self.forward(p, 0)

    def relay(self, p):
        for d, copy in enumerate(self.along[p]):
            copy.wait_recv()
            self.forward(p, d + 1)

    def finish(self, p):
        for copy in self.across[p]:
            copy.wait_recv()
        blocks = [
            self.buf[p, z, y].astype(F32) for z in range(self.n_z) for y in range(PAIR)
        ]
        return jnp.concatenate(blocks, axis=0).astype(BF16)

    def drain(self):
        for p in self.along:
            for copy in self.along[p] + self.across[p]:
                copy.wait_send()


def fused_kernel(sizes, rate_ref, x_hbm, mg_hbm, cg_hbm, *refs):
    n_kv, n_tp, rows, width, dk, dv, heads, dim = sizes
    (qw_hbm, kw_hbm, vw_hbm, gw_hbm, ow_hbm, up_hbm, down_hbm, old_hbm) = refs[:8]
    (out_ref, k_ref, v_ref, held) = refs[8:12]
    (pack, gain_in, qw, kw, vw, gw, ow, up, down) = refs[12:21]
    (part, got, summed, got2, part_u, got_u, summed_u, got2_u) = refs[21:29]
    (sq_src, sq_dst, sq_src2, sq_dst2, mixes, hid, ret, acc) = refs[29:37]
    (pair_own, pair_got, chip, far, mids, ends, got_ends) = refs[37:44]
    (w_sem, s_sem, in_sem, t_sem, sq_sem, sq_sem2) = refs[44:50]
    (sem_a, sem_b, sem_ua, sem_ub, mz_sem, my_sem, hz_sem, hy_sem) = refs[50:58]
    (c_sem, far_sem, f_sem) = refs[58:61]
    kv, tp = lax.axis_index("kv"), lax.axis_index("tp")
    z, y = lax.div(kv, PAIR), lax.rem(kv, PAIR)
    n_x = n_tp // CORES
    cx, core = lax.div(tp, CORES), lax.rem(tp, CORES)
    batch, block = x_hbm.shape
    loads = {}

    def load(name, src, dst, sem):
        loads[name] = pltpu.make_async_copy(src, dst, sem)
        loads[name].start()

    load("x", x_hbm, pack.at[tp, pl.ds(0, batch)], in_sem.at[0])
    load("mg", mg_hbm, gain_in.at[0], in_sem.at[1])
    load("cg", cg_hbm, gain_in.at[1], in_sem.at[2])
    for i, (name, src, dst) in enumerate(
        [("q", qw_hbm, qw), ("k", kw_hbm, kw), ("v", vw_hbm, vw), ("g", gw_hbm, gw)]
    ):
        load(name, src, dst, w_sem.at[i])
    barrier = pltpu.get_barrier_semaphore()
    for d in range(1, n_kv):
        pl.semaphore_signal(
            barrier, inc=1, device_id={"kv": lax.rem(kv + d, n_kv)}, device_id_type=MESH
        )
    for d in range(1, n_tp):
        pl.semaphore_signal(
            barrier, inc=1, device_id={"tp": lax.rem(tp + d, n_tp)}, device_id_type=MESH
        )
    for name in ("x", "mg", "cg"):
        loads[name].wait()
    for i in range(2):
        gain = jnp.broadcast_to(gain_in[i].astype(F32), (GAIN_ROWS, block))
        pack[tp, batch + i * GAIN_ROWS : batch + (i + 1) * GAIN_ROWS] = gain.astype(BF16)
    pl.semaphore_wait(barrier, n_tp + n_kv - 2)
    x_copies = tp_gather(pack, tp, n_tp, t_sem)
    load("old", old_hbm, held, s_sem)
    for copy in x_copies:
        copy.wait_recv()

    def normalise(stream, row):
        parts = [
            (stream[t] * pack[t, row : row + GAIN_ROWS][:1].astype(F32)).astype(BF16)
            for t in range(n_tp)
        ]
        return jnp.concatenate(parts, axis=1)

    def squares_of(stream):
        return sum(jnp.sum(s * s, axis=1, keepdims=True) for s in stream)

    stream = [pack[t, :batch].astype(F32) for t in range(n_tp)]
    normed = normalise(stream, batch)
    sq_copies, sq_total = own_square_total(
        squares_of(stream), sq_src, sq_dst, kv, n_kv, rows, sq_sem
    )
    scatter = PairScatter(kv, n_kv, rows, part, got, summed, got2, sem_a, sem_b)
    mix_gather = PairGather(kv, n_kv, mixes, mz_sem, my_sem)

    def project(p):
        h, kind = divmod(p, 3)
        if h == 0:
            for name in (("q", "k"), ("v",), ("g",))[kind]:
                loads[name].wait()
        if kind == 0:
            cols = slice(h * dk, (h + 1) * dk)
            return jnp.concatenate(
                [
                    jnp.dot(normed, qw[:, cols], preferred_element_type=F32),
                    jnp.dot(normed, kw[:, cols], preferred_element_type=F32),
                ],
                axis=1,
            )
        w = (vw, gw)[kind - 1]
        return jnp.dot(normed, w[:, h * dv : (h + 1) * dv], preferred_element_type=F32)

    def retain(h, query, key, value, gate):
        columns = query.T
        step = min(dk, 64)
        for s in range(rows):
            total = jnp.zeros((8, dv), F32)
            for r in range(0, dk, step):
                term = columns[r : r + step, s : s + 1] * held[s, h, r : r + step]
                total = total + jnp.sum(term.reshape(step // 8, 8, dv), axis=0)
            ret[s : s + 1] = jnp.sum(total, axis=0, keepdims=True)
        out = rate_ref[h] * ret[...] + jnp.sum(query * key, axis=1, keepdims=True) * value
        out = out * lax.rsqrt(jnp.mean(out * out, axis=1, keepdims=True) + EPS)
        mixes[h, z, y] = (jax.nn.silu(gate) * out).astype(BF16)

    def attend(h):
        if h == 0:
            loads["ow"].wait()
        term = jnp.dot(
            mix_gather.finish(h), ow[h * dv : (h + 1) * dv], preferred_element_type=F32
        )
        acc[...] = term if h == 0 else acc[...] + term

    pieces = 3 * heads
    scale, values = None, {}
    for s in range(pieces + LAG_A + LAG_B):
        if s < pieces:
            scatter.start(s, project(s))
        if s == 0:
            load("ow", ow_hbm, ow, w_sem.at[4])
            load("up", up_hbm, up, w_sem.at[5])
            load("down", down_hbm, down, w_sem.at[6])
        p = s - LAG_A
        if 0 <= p < pieces:
            scatter.middle(p)
        p = p - LAG_B
        if 0 <= p < pieces:
            if p == 0:
                scale = lax.rsqrt(sq_total() / dim + EPS)
            h, kind = divmod(p, 3)
            total = scatter.finish(p) * scale
            if kind == 0:
                query, key = total[:, :dk], total[:, dk:] * dk ** (-0.5)
                k_ref[:, h * dk : (h + 1) * dk] = key
                values["q"], values["k"] = query, key
            elif kind == 1:
                v_ref[:, h * dv : (h + 1) * dv] = total
                values["v"] = total
            else:
                if h == 0:
                    loads["old"].wait()
                retain(h, values["q"], values["k"], values["v"], total)
                mix_gather.start(h)
                if h >= 1:
                    mix_gather.relay(h - 1)
                if h >= 2:
                    attend(h - 2)
    mix_gather.relay(heads - 1)
    for h in range(max(heads - 2, 0), heads):
        attend(h)

    half = pair_own.shape[1] // 2
    pair_own[...] = acc[...].astype(BF16)
    pair_copy = put(
        pair_own, pair_got, c_sem.at[0], c_sem.at[1], {"tp": cx * CORES + 1 - core}
    )
    pair_copy.wait_recv()
    both = pair_own[...].astype(F32) + pair_got[...].astype(F32)
    for j in range(CORES):
        chip[j] = both[:, j * half : (j + 1) * half].astype(BF16)
    far_copies = []
    for d in range(1, n_x):
        for rel in range(CORES):
            peer = lax.rem(cx + d, n_x) * CORES + lax.rem(core + rel, CORES)
            far_copies.append(
                put(
                    chip.at[core],
                    far.at[d - 1, rel],
                    far_sem.at[0, d - 1, rel],
                    far_sem.at[1, d - 1, rel],
                    {"tp": peer},
                )
            )
    for copy in far_copies:
        copy.wait_recv()
    sums = []
    for j in range(CORES):
        total = chip[j].astype(F32)
        for d in range(n_x - 1):
            total = total + far[d, lax.rem(core + j, CORES)].astype(F32)
        sums.append(total)
    attention = jnp.concatenate(sums, axis=1)
    for t in range(n_tp):
        mids[t] = (
            pack[t, :batch].astype(F32) + attention[:, t * block : (t + 1) * block]
        ).astype(BF16)
    stream = [mids[t].astype(F32) for t in range(n_tp)]
    normed_mid = normalise(stream, batch + GAIN_ROWS)
    sq_copies2, sq_total2 = own_square_total(
        squares_of(stream), sq_src2, sq_dst2, kv, n_kv, rows, sq_sem2
    )
    lift = PairScatter(kv, n_kv, rows, part_u, got_u, summed_u, got2_u, sem_ua, sem_ub)
    gather = PairGather(kv, n_kv, hid, hz_sem, hy_sem)
    count = up.shape[1] // width
    loads["up"].wait()
    scale2 = None
    for s in range(count + LAG_1 + LAG_2 + LAG_3 + LAG_4):
        if s < count:
            w = up[:, s * width : (s + 1) * width]
            lift.start(s, jnp.dot(normed_mid, w, preferred_element_type=F32))
        p = s - LAG_1
        if 0 <= p < count:
            lift.middle(p)
        p = p - LAG_2
        if 0 <= p < count:
            if p == 0:
                scale2 = lax.rsqrt(sq_total2() / dim + EPS)
            lifted = lift.finish(p) * scale2
            hid[p, z, y] = jnp.square(jnp.maximum(lifted, 0.0)).astype(BF16)
            gather.start(p)
        p = p - LAG_3
        if 0 <= p < count:
            gather.relay(p)
        p = p - LAG_4
        if 0 <= p < count:
            if p == 0:
                loads["down"].wait()
            w = down[p * width : (p + 1) * width]
            term = jnp.dot(gather.finish(p), w, preferred_element_type=F32)
            acc[...] = term if p == 0 else acc[...] + term
    for t in range(n_tp):
        ends[t] = acc[:, t * block : (t + 1) * block].astype(BF16)
    f_copies = tp_scatter(ends, got_ends, tp, n_tp, f_sem)
    lowered = ends[tp].astype(F32)
    for d, copy in enumerate(f_copies):
        copy.wait_recv()
        lowered = lowered + got_ends[d].astype(F32)
    out_ref[...] = (mids[tp].astype(F32) + lowered).astype(BF16)
    for group in (scatter, mix_gather, lift, gather):
        group.drain()
    rest = x_copies + sq_copies + sq_copies2 + far_copies + f_copies
    for copy in rest + [pair_copy]:
        copy.wait_send()


def state_kernel(heads, dk, dv, k_ref, v_ref, act_ref, rate_ref, old_ref, *refs):
    act_out, out_ref, new_ref, sem, act_sem = refs
    step = min(dk, 64)
    seqs = k_ref.shape[0]
    act_copy = pltpu.make_async_copy(act_ref, act_out, act_sem)
    act_copy.start()

    def write(s, h):
        return pltpu.make_async_copy(new_ref.at[s, h], out_ref.at[s, h], sem.at[s, h])

    def one(s, carry):
        k_row = k_ref[pl.ds(s, 1), :]
        lines = [k_row[:, h * dk : (h + 1) * dk] for h in range(heads)]
        lines.append(jnp.zeros((-heads % 8, dk), F32))
        columns = jnp.concatenate(lines, axis=0).T
        for h in range(heads):
            value = v_ref[pl.ds(s, 1), h * dv : (h + 1) * dv]
            for r in range(0, dk, step):
                key = columns[r : r + step, h : h + 1]
                new_ref[s, h, r : r + step] = (
                    rate_ref[h] * old_ref[s, h, r : r + step] + key * value
                )
            write(s, h).start()
        return carry

    lax.fori_loop(0, seqs, one, 0, unroll=2)
    for s in range(seqs):
        for h in range(heads):
            write(s, h).wait()
    act_copy.wait()


def in_hbm(a):
    return pltpu.with_memory_space_constraint(a, pltpu.HBM)


VM = pl.BlockSpec(memory_space=pltpu.VMEM)
SM = pl.BlockSpec(memory_space=pltpu.SMEM)
ANY = pl.BlockSpec(memory_space=pltpu.HBM)


def scatter_scratch(count, n_kv, rows, width):
    n_z = n_kv // PAIR
    return [
        pltpu.VMEM((count, PAIR, n_z, rows, width), BF16),
        pltpu.VMEM((count, n_z, rows, width), BF16),
        pltpu.VMEM((count, n_z, rows, width), BF16),
        pltpu.VMEM((count, n_z - 1, rows, width), BF16),
    ]


def fused_device(n_kv, n_tp, x, mg, cg, qw, kw, vw, gw, ow, uw, dw, state):
    seqs, heads, dk, dv = state.shape
    batch, block = x.shape
    dim = block * n_kv * n_tp
    n_z, n_x = n_kv // PAIR, n_tp // CORES
    depth, cols = qw.shape[0], ow.shape[1]
    width = min(WIDTH, uw.shape[1])
    count, pieces = uw.shape[1] // width, 3 * heads
    rates = lax.dynamic_slice_in_dim(
        head_decays(HEADS), lax.axis_index("tp") * heads, heads, 0
    )
    elements = sum(w.size for w in (qw, kw, vw, gw, ow, uw, dw))
    out, key, value, held = pl.pallas_call(
        functools.partial(fused_kernel, (n_kv, n_tp, seqs, width, dk, dv, heads, dim)),
        out_shape=[
            jax.ShapeDtypeStruct((batch, block), BF16),
            jax.ShapeDtypeStruct((seqs, heads * dk), F32),
            jax.ShapeDtypeStruct((seqs, heads * dv), F32),
            pltpu.VMEM(state.shape, F32),
        ],
        in_specs=[SM] + [ANY] * 11,
        out_specs=[VM] * 4,
        scratch_shapes=[
            pltpu.VMEM((n_tp, batch + 2 * GAIN_ROWS, block), BF16),
            pltpu.VMEM((2, 1, block), BF16),
            *[pltpu.VMEM(w.shape, BF16) for w in (qw, kw, vw, gw, ow, uw, dw)],
            *scatter_scratch(pieces, n_kv, seqs, dv),
            *scatter_scratch(count, n_kv, seqs, width),
            pltpu.VMEM((n_kv, seqs, 128), F32),
            pltpu.VMEM((n_kv - 1, seqs, 128), F32),
            pltpu.VMEM((n_kv, seqs, 128), F32),
            pltpu.VMEM((n_kv - 1, seqs, 128), F32),
            pltpu.VMEM((heads, n_z, PAIR, seqs, dv), BF16),
            pltpu.VMEM((count, n_z, PAIR, seqs, width), BF16),
            pltpu.VMEM((seqs, dv), F32),
            pltpu.VMEM((batch, cols), F32),
            pltpu.VMEM((batch, cols), BF16),
            pltpu.VMEM((batch, cols), BF16),
            pltpu.VMEM((CORES, batch, cols // CORES), BF16),
            pltpu.VMEM((max(n_x - 1, 1), CORES, batch, cols // CORES), BF16),
            pltpu.VMEM((n_tp, batch, block), BF16),
            pltpu.VMEM((n_tp, batch, block), BF16),
            pltpu.VMEM((n_tp - 1, batch, block), BF16),
            DMA((7,)),
            DMA,
            DMA((3,)),
            DMA((2, n_tp - 1)),
            DMA((2, n_kv - 1)),
            DMA((2, n_kv - 1)),
            DMA((2, pieces)),
            DMA((2, pieces, n_z - 1)),
            DMA((2, count)),
            DMA((2, count, n_z - 1)),
            DMA((2, heads, n_z - 1)),
            DMA((2, heads, n_z)),
            DMA((2, count, n_z - 1)),
            DMA((2, count, n_z)),
            DMA((2,)),
            DMA((2, max(n_x - 1, 1), CORES)),
            DMA((2, n_tp - 1)),
        ],
        compiler_params=pltpu.CompilerParams(
            collective_id=0, has_side_effects=True, vmem_limit_bytes=26 * 2**20
        ),
        cost_estimate=pl.CostEstimate(
            flops=2 * batch * elements,
            bytes_accessed=2 * elements + 4 * state.size,
            transcendentals=0,
        ),
        name="fused",
    )(
        rates,
        *[in_hbm(a) for a in (x, mg.reshape(1, block), cg.reshape(1, block))],
        *[in_hbm(a) for a in (qw, kw, vw, gw, ow, uw, dw, state)],
    )
    return pl.pallas_call(
        functools.partial(state_kernel, heads, dk, dv),
        out_shape=[pltpu.HBM((batch, block), BF16), pltpu.HBM(state.shape, F32)],
        in_specs=[VM, VM, VM, SM, VM],
        out_specs=[ANY, ANY],
        scratch_shapes=[pltpu.VMEM(state.shape, F32), DMA((seqs, heads)), DMA],
        compiler_params=pltpu.CompilerParams(vmem_limit_bytes=18 * 2**20),
        cost_estimate=pl.CostEstimate(
            flops=3 * state.size, bytes_accessed=8 * state.size, transcendentals=0
        ),
        name="state",
    )(key, value, out, rates, held)


def solution(mesh):
    return jax.shard_map(
        functools.partial(fused_device, mesh.shape["kv"], mesh.shape["tp"]),
        mesh=mesh,
        in_specs=(
            P(None, ("kv", "tp")),
            P(("kv", "tp")),
            P(("kv", "tp")),
            P("kv", "tp"),
            P("kv", "tp"),
            P("kv", "tp"),
            P("kv", "tp"),
            P("tp", "kv"),
            P("kv", "tp"),
            P("tp", "kv"),
            P("kv", "tp", None, None),
        ),
        out_specs=(P(None, ("kv", "tp")), P("kv", "tp", None, None)),
        check_vma=False,
    )
```

time: 77.5 us -> 73.8 us (0.952)
  local copies, waits for them, and re-layouts: 2.07 us -> 0.08 us
  Pallas kernels: 74.4 us -> 72.9 us
    unnamed x9 -> x0, local copies, waits for them, and re-layouts: 1.99 us -> none
    pallas_call x3 -> x2, Pallas kernels: 74.4 us -> 72.9 us  [the longest x1 66 us: fused_device(): pl.pallas_call(functools.partial(fused_kernel, (n_kv, n_tp, seqs, width,...]
where the time goes in v1:
time: 73.8 us; the launch traced here: 73.7 us
  Pallas kernels  72.9 us (99%)
    pallas_call x1, Pallas kernels, fused_device(): pl.pallas_call(functools.partial(fused_kernel, (n_kv, n_tp, seqs, width,...  66 us
    pallas_call x1, Pallas kernels, fused_device(): pl.pallas_call(functools.partial(state_kernel, heads, dk, dv), out_shape=...  6.97 us

profile of v1, /device:TPU:0, one launch (start us, length us, event | category | flops | bytes accessed | tf_op | source)
XLA Modules:
  0.0 73.7 jit_solution(3998759183329136335)
XLA Ops:
  0.6 0.1 dynamic_slice.3.rate_ref
  0.7 66.0 %fused.1 = (bf16[64,128]{1,0:T(8,128)(2,1)S(1)}, f32[8,1024]{1,0:T(8,128)S(1)}, f32[8,2048]{1,0:T(8,128)S(1)}, f32[8,4,256,512]{3,2,1,0:T(8,128)S(1)}) custom-call(f32[4]{0:T(128)S(1)} %dynamic_slice.3.rate_ref, bf16[64,128]{1,0:T(8,128)(2,1)} %x_hbm.1, bf16[1,128]{1,0:T(2,128)(2,1)} %bitcast.2, bf16[1,128]{1,0:T(2,128)(2,1)} %bitcast.3, ...), custom_call_target="tpu_custom_call" | custom-call | flops 1073741824 | bytes 33554432 | tf_op jit(solution)/shard_map/fused/pallas_call | solution.py:489
  66.7 7.0 %state.1 = (bf16[64,128]{1,0:T(8,128)(2,1)}, f32[8,4,256,512]{3,2,1,0:T(8,128)}) custom-call(f32[8,1024]{1,0:T(8,128)S(1)} %get-tuple-element.6.k_ref, f32[8,2048]{1,0:T(8,128)S(1)} %get-tuple-element.7.v_ref, bf16[64,128]{1,0:T(8,128)(2,1)S(1)} %get-tuple-element.8.act_ref, f32[4]{0:T(128)S(1)} %dynamic_slice.3.rate_ref, ...), custom_call_target="tpu_custom_call" | custom-call | flops 12582912 | bytes 33554432 | tf_op jit(solution)/shard_map/state/pallas_call | solution.py:552
  (1 shorter events, 0.0 us)

commit v2 on v1

--- a/solution.py
+++ b/solution.py
@@ -39,62 +39,45 @@
     return copy
 
 
+def landed(ref, sem):
+    pltpu.make_async_copy(ref, ref, sem).wait()
+
+
 def tp_gather(buf, tp, n_tp, sems):
-    return [
-        put(
-            buf.at[tp],
-            buf.at[tp],
-            sems.at[0, d - 1],
-            sems.at[1, d - 1],
-            {"tp": lax.rem(tp + d, n_tp)},
-        )
-        for d in range(1, n_tp)
-    ]
+    for d in range(1, n_tp):
+        put(buf.at[tp], buf.at[tp], sems.at[0], sems.at[1], {"tp": lax.rem(tp + d, n_tp)})
 
 
 def tp_scatter(src, dst, tp, n_tp, sems):
-    copies = []
     for d in range(1, n_tp):
         peer = lax.rem(tp + d, n_tp)
-        copies.append(
-            put(src.at[peer], dst.at[d - 1], sems.at[0, d - 1], sems.at[1, d - 1], {"tp": peer})
-        )
-    return copies
-
-
-def kv_scatter_small(src, dst, kv, n_kv, sems):
-    copies = []
+        put(src.at[peer], dst.at[d - 1], sems.at[0], sems.at[1], {"tp": peer})
+
+
+def square_total(squares, sq_src, sq_dst, kv, n_kv, rows, sems):
+    for g in range(n_kv):
+        sq_src[g] = jnp.broadcast_to(squares[g * rows : (g + 1) * rows], sq_src.shape[1:])
     for d in range(1, n_kv):
         peer = lax.rem(kv + d, n_kv)
-        copies.append(
-            put(src.at[peer], dst.at[d - 1], sems.at[0, d - 1], sems.at[1, d - 1], {"kv": peer})
-        )
-    return copies
-
-
-def own_square_total(squares, sq_src, sq_dst, kv, n_kv, rows, sems):
-    for g in range(n_kv):
-        sq_src[g] = jnp.broadcast_to(squares[g * rows : (g + 1) * rows], sq_src.shape[1:])
-    copies = kv_scatter_small(sq_src, sq_dst, kv, n_kv, sems)
+        put(sq_src.at[peer], sq_dst.at[d - 1], sems.at[0], sems.at[1], {"kv": peer})
 
     def finish():
+        landed(sq_dst, sems.at[1])
         total = sq_src[kv]
-        for d, copy in enumerate(copies):
-            copy.wait_recv()
+        for d in range(n_kv - 1):
             total = total + sq_dst[d]
         return total[:, :1]
 
-    return copies, finish
+    return finish
 
 
 class PairScatter:
-    def __init__(self, kv, n_kv, rows, part, got, summed, got2, sem_a, sem_b):
+    def __init__(self, kv, n_kv, rows, part, got, summed, got2, sends, sem_a, sem_b):
         self.n_z = n_kv // PAIR
         self.z, self.y = lax.div(kv, PAIR), lax.rem(kv, PAIR)
         self.rows = rows
         self.part, self.got, self.summed, self.got2 = part, got, summed, got2
-        self.sem_a, self.sem_b = sem_a, sem_b
-        self.first, self.second = {}, {}
+        self.sends, self.sem_a, self.sem_b = sends, sem_a, sem_b
 
     def start(self, p, value):
         rows = self.rows
@@ -103,97 +86,71 @@
                 at = (z * PAIR + y) * rows
                 self.part[p, y, z] = value[at : at + rows].astype(BF16)
         other = 1 - self.y
-        self.first[p] = put(
+        put(
             self.part.at[p, other],
             self.got.at[p],
-            self.sem_a.at[0, p],
-            self.sem_a.at[1, p],
+            self.sends.at[0],
+            self.sem_a.at[p],
             {"kv": self.z * PAIR + other},
         )
 
     def middle(self, p):
-        self.first[p].wait_recv()
+        landed(self.got.at[p], self.sem_a.at[p])
         self.summed[p] = (self.part[p, self.y].astype(F32) + self.got[p].astype(F32)).astype(BF16)
-        copies = []
         for d in range(1, self.n_z):
             peer = lax.rem(self.z + d, self.n_z)
-            copies.append(
-                put(
-                    self.summed.at[p, peer],
-                    self.got2.at[p, d - 1],
-                    self.sem_b.at[0, p, d - 1],
-                    self.sem_b.at[1, p, d - 1],
-                    {"kv": peer * PAIR + self.y},
-                )
+            put(
+                self.summed.at[p, peer],
+                self.got2.at[p, d - 1],
+                self.sends.at[1],
+                self.sem_b.at[p],
+                {"kv": peer * PAIR + self.y},
             )
-        self.second[p] = copies
 
     def finish(self, p):
+        landed(self.got2.at[p], self.sem_b.at[p])
         total = self.summed[p, self.z].astype(F32)
-        for d, copy in enumerate(self.second[p]):
-            copy.wait_recv()
+        for d in range(self.n_z - 1):
             total = total + self.got2[p, d].astype(F32)
         return total
 
     def drain(self):
-        for p in self.first:
-            self.first[p].wait_send()
-            for copy in self.second[p]:
-                copy.wait_send()
+        landed(self.got, self.sends.at[0])
+        landed(self.got2, self.sends.at[1])
 
 
 class PairGather:
-    def __init__(self, kv, n_kv, buf, sem_z, sem_y):
+    def __init__(self, kv, n_kv, buf, sends, sem_z, sem_y):
         self.n_z = n_kv // PAIR
         self.z, self.y = lax.div(kv, PAIR), lax.rem(kv, PAIR)
-        self.buf, self.sem_z, self.sem_y = buf, sem_z, sem_y
-        self.along, self.across = {}, {}
-
-    def forward(self, p, d):
-        z = lax.rem(self.z - d + self.n_z, self.n_z)
-        self.across[p].append(
-            put(
-                self.buf.at[p, z, self.y],
-                self.buf.at[p, z, self.y],
-                self.sem_y.at[0, p, d],
-                self.sem_y.at[1, p, d],
-                {"kv": self.z * PAIR + 1 - self.y},
-            )
-        )
+        self.buf, self.sends, self.sem_z, self.sem_y = buf, sends, sem_z, sem_y
 
     def start(self, p):
         own = self.buf.at[p, self.z, self.y]
-        self.along[p], self.across[p] = [], []
         for d in range(1, self.n_z):
             peer = lax.rem(self.z + d, self.n_z)
-            self.along[p].append(
-                put(
-                    own,
-                    own,
-                    self.sem_z.at[0, p, d - 1],
-                    self.sem_z.at[1, p, d - 1],
-                    {"kv": peer * PAIR + self.y},
-                )
-            )
-        self.forward(p, 0)
+            put(own, own, self.sends.at[0], self.sem_z.at[p], {"kv": peer * PAIR + self.y})
 
     def relay(self, p):
-        for d, copy in enumerate(self.along[p]):
-            copy.wait_recv()
-            self.forward(p, d + 1)
+        landed(self.buf.at[p, pl.ds(0, self.n_z - 1), 0], self.sem_z.at[p])
+        put(
+            self.buf.at[p, :, self.y],
+            self.buf.at[p, :, self.y],
+            self.sends.at[1],
+            self.sem_y.at[p],
+            {"kv": self.z * PAIR + 1 - self.y},
+        )
 
     def finish(self, p):
-        for copy in self.across[p]:
-            copy.wait_recv()
+        landed(self.buf.at[p, :, 0], self.sem_y.at[p])
         blocks = [
             self.buf[p, z, y].astype(F32) for z in range(self.n_z) for y in range(PAIR)
         ]
         return jnp.concatenate(blocks, axis=0).astype(BF16)
 
     def drain(self):
-        for p in self.along:
-            for copy in self.along[p] + self.across[p]:
-                copy.wait_send()
+        landed(self.buf.at[:, pl.ds(0, self.n_z - 1), 0], self.sends.at[0])
+        landed(self.buf.at[:, :, 0], self.sends.at[1])
 
 
 def fused_kernel(sizes, rate_ref, x_hbm, mg_hbm, cg_hbm, *refs):
@@ -206,7 +163,7 @@
     (pair_own, pair_got, chip, far, mids, ends, got_ends) = refs[37:44]
     (w_sem, s_sem, in_sem, t_sem, sq_sem, sq_sem2) = refs[44:50]
     (sem_a, sem_b, sem_ua, sem_ub, mz_sem, my_sem, hz_sem, hy_sem) = refs[50:58]
-    (c_sem, far_sem, f_sem) = refs[58:61]
+    (c_sem, far_sem, f_sem, s_send, u_send, m_send, h_send) = refs[58:65]
     kv, tp = lax.axis_index("kv"), lax.axis_index("tp")
     z, y = lax.div(kv, PAIR), lax.rem(kv, PAIR)
     n_x = n_tp // CORES
@@ -218,13 +175,6 @@
         loads[name] = pltpu.make_async_copy(src, dst, sem)
         loads[name].start()
 
-    load("x", x_hbm, pack.at[tp, pl.ds(0, batch)], in_sem.at[0])
-    load("mg", mg_hbm, gain_in.at[0], in_sem.at[1])
-    load("cg", cg_hbm, gain_in.at[1], in_sem.at[2])
-    for i, (name, src, dst) in enumerate(
-        [("q", qw_hbm, qw), ("k", kw_hbm, kw), ("v", vw_hbm, vw), ("g", gw_hbm, gw)]
-    ):
-        load(name, src, dst, w_sem.at[i])
     barrier = pltpu.get_barrier_semaphore()
     for d in range(1, n_kv):
         pl.semaphore_signal(
@@ -234,16 +184,22 @@
         pl.semaphore_signal(
             barrier, inc=1, device_id={"tp": lax.rem(tp + d, n_tp)}, device_id_type=MESH
         )
+    load("x", x_hbm, pack.at[tp, pl.ds(0, batch)], in_sem.at[0])
+    load("mg", mg_hbm, gain_in.at[0], in_sem.at[1])
+    load("cg", cg_hbm, gain_in.at[1], in_sem.at[2])
     for name in ("x", "mg", "cg"):
         loads[name].wait()
+    for i, (name, src, dst) in enumerate(
+        [("q", qw_hbm, qw), ("k", kw_hbm, kw), ("v", vw_hbm, vw), ("g", gw_hbm, gw)]
+    ):
+        load(name, src, dst, w_sem.at[i])
     for i in range(2):
         gain = jnp.broadcast_to(gain_in[i].astype(F32), (GAIN_ROWS, block))
         pack[tp, batch + i * GAIN_ROWS : batch + (i + 1) * GAIN_ROWS] = gain.astype(BF16)
     pl.semaphore_wait(barrier, n_tp + n_kv - 2)
-    x_copies = tp_gather(pack, tp, n_tp, t_sem)
+    tp_gather(pack, tp, n_tp, t_sem)
     load("old", old_hbm, held, s_sem)
-    for copy in x_copies:
-        copy.wait_recv()
+    landed(pack.at[pl.ds(0, n_tp - 1)], t_sem.at[1])
 
     def normalise(stream, row):
         parts = [
@@ -257,11 +213,9 @@
 
     stream = [pack[t, :batch].astype(F32) for t in range(n_tp)]
     normed = normalise(stream, batch)
-    sq_copies, sq_total = own_square_total(
-        squares_of(stream), sq_src, sq_dst, kv, n_kv, rows, sq_sem
-    )
-    scatter = PairScatter(kv, n_kv, rows, part, got, summed, got2, sem_a, sem_b)
-    mix_gather = PairGather(kv, n_kv, mixes, mz_sem, my_sem)
+    sq_total = square_total(squares_of(stream), sq_src, sq_dst, kv, n_kv, rows, sq_sem)
+    scatter = PairScatter(kv, n_kv, rows, part, got, summed, got2, s_send, sem_a, sem_b)
+    mix_gather = PairGather(kv, n_kv, mixes, m_send, mz_sem, my_sem)
 
     def project(p):
         h, kind = divmod(p, 3)
@@ -331,10 +285,11 @@
                     loads["old"].wait()
                 retain(h, values["q"], values["k"], values["v"], total)
                 mix_gather.start(h)
-                if h >= 1:
-                    mix_gather.relay(h - 1)
-                if h >= 2:
-                    attend(h - 2)
+                if h == heads - 1:
+                    for g in range(max(heads - 1, 0)):
+                        mix_gather.relay(g)
+                    for g in range(max(heads - 2, 0)):
+                        attend(g)
     mix_gather.relay(heads - 1)
     for h in range(max(heads - 2, 0), heads):
         attend(h)
@@ -348,21 +303,17 @@
     both = pair_own[...].astype(F32) + pair_got[...].astype(F32)
     for j in range(CORES):
         chip[j] = both[:, j * half : (j + 1) * half].astype(BF16)
-    far_copies = []
     for d in range(1, n_x):
         for rel in range(CORES):
             peer = lax.rem(cx + d, n_x) * CORES + lax.rem(core + rel, CORES)
-            far_copies.append(
-                put(
-                    chip.at[core],
-                    far.at[d - 1, rel],
-                    far_sem.at[0, d - 1, rel],
-                    far_sem.at[1, d - 1, rel],
-                    {"tp": peer},
-                )
+            put(
+                chip.at[core],
+                far.at[d - 1, rel],
+                far_sem.at[0],
+                far_sem.at[1],
+                {"tp": peer},
             )
-    for copy in far_copies:
-        copy.wait_recv()
+    landed(far, far_sem.at[1])
     sums = []
     for j in range(CORES):
         total = chip[j].astype(F32)
@@ -376,11 +327,11 @@
         ).astype(BF16)
     stream = [mids[t].astype(F32) for t in range(n_tp)]
     normed_mid = normalise(stream, batch + GAIN_ROWS)
-    sq_copies2, sq_total2 = own_square_total(
-        squares_of(stream), sq_src2, sq_dst2, kv, n_kv, rows, sq_sem2
+    sq_total2 = square_total(squares_of(stream), sq_src2, sq_dst2, kv, n_kv, rows, sq_sem2)
+    lift = PairScatter(
+        kv, n_kv, rows, part_u, got_u, summed_u, got2_u, u_send, sem_ua, sem_ub
     )
-    lift = PairScatter(kv, n_kv, rows, part_u, got_u, summed_u, got2_u, sem_ua, sem_ub)
-    gather = PairGather(kv, n_kv, hid, hz_sem, hy_sem)
+    gather = PairGather(kv, n_kv, hid, h_send, hz_sem, hy_sem)
     count = up.shape[1] // width
     loads["up"].wait()
     scale2 = None
@@ -410,17 +361,20 @@
             acc[...] = term if p == 0 else acc[...] + term
     for t in range(n_tp):
         ends[t] = acc[:, t * block : (t + 1) * block].astype(BF16)
-    f_copies = tp_scatter(ends, got_ends, tp, n_tp, f_sem)
+    tp_scatter(ends, got_ends, tp, n_tp, f_sem)
+    landed(got_ends, f_sem.at[1])
     lowered = ends[tp].astype(F32)
-    for d, copy in enumerate(f_copies):
-        copy.wait_recv()
+    for d in range(n_tp - 1):
         lowered = lowered + got_ends[d].astype(F32)
     out_ref[...] = (mids[tp].astype(F32) + lowered).astype(BF16)
     for group in (scatter, mix_gather, lift, gather):
         group.drain()
-    rest = x_copies + sq_copies + sq_copies2 + far_copies + f_copies
-    for copy in rest + [pair_copy]:
-        copy.wait_send()
+    pair_copy.wait_send()
+    landed(pack.at[pl.ds(0, n_tp - 1)], t_sem.at[0])
+    landed(sq_dst, sq_sem.at[0])
+    landed(sq_dst2, sq_sem2.at[0])
+    landed(far, far_sem.at[0])
+    landed(got_ends, f_sem.at[0])
 
 
 def state_kernel(heads, dk, dv, k_ref, v_ref, act_ref, rate_ref, old_ref, *refs):
@@ -520,20 +474,12 @@
             DMA((7,)),
             DMA,
             DMA((3,)),
-            DMA((2, n_tp - 1)),
-            DMA((2, n_kv - 1)),
-            DMA((2, n_kv - 1)),
-            DMA((2, pieces)),
-            DMA((2, pieces, n_z - 1)),
-            DMA((2, count)),
-            DMA((2, count, n_z - 1)),
-            DMA((2, heads, n_z - 1)),
-            DMA((2, heads, n_z)),
-            DMA((2, count, n_z - 1)),
-            DMA((2, count, n_z)),
-            DMA((2,)),
-            DMA((2, max(n_x - 1, 1), CORES)),
-            DMA((2, n_tp - 1)),
+            *[DMA((2,))] * 3,
+            *[DMA((pieces,))] * 2,
+            *[DMA((count,))] * 2,
+            *[DMA((heads,))] * 2,
+            *[DMA((count,))] * 2,
+            *[DMA((2,))] * 7,
         ],
         compiler_params=pltpu.CompilerParams(
             collective_id=0, has_side_effects=True, vmem_limit_bytes=26 * 2**20

time: 73.8 us -> 70.5 us (0.955)
  Pallas kernels: 72.9 us -> 69.5 us
    pallas_call x1, Pallas kernels: 66 us -> 62.5 us  [fused_device(): pl.pallas_call(functools.partial(fused_kernel, (n_kv, n_tp, seqs, width,...]
where the time goes in v2:
time: 70.5 us; the launch traced here: 70.2 us
  Pallas kernels  69.5 us (99%)
    pallas_call x1, Pallas kernels, fused_device(): pl.pallas_call(functools.partial(fused_kernel, (n_kv, n_tp, seqs, width,...  62.5 us
    pallas_call x1, Pallas kernels, fused_device(): pl.pallas_call(functools.partial(state_kernel, heads, dk, dv), out_shape=...  6.97 us

profile of v2, /device:TPU:0, one launch (start us, length us, event | category | flops | bytes accessed | tf_op | source)
XLA Modules:
  0.0 70.2 jit_solution(4531947711378750695)
XLA Ops:
  0.6 0.1 dynamic_slice.3.rate_ref
  0.7 62.5 %fused.1 = (bf16[64,128]{1,0:T(8,128)(2,1)S(1)}, f32[8,1024]{1,0:T(8,128)S(1)}, f32[8,2048]{1,0:T(8,128)S(1)}, f32[8,4,256,512]{3,2,1,0:T(8,128)S(1)}) custom-call(f32[4]{0:T(128)S(1)} %dynamic_slice.3.rate_ref, bf16[64,128]{1,0:T(8,128)(2,1)} %x_hbm.1, bf16[1,128]{1,0:T(2,128)(2,1)} %bitcast.2, bf16[1,128]{1,0:T(2,128)(2,1)} %bitcast.3, ...), custom_call_target="tpu_custom_call" | custom-call | flops 1073741824 | bytes 33554432 | tf_op jit(solution)/shard_map/fused/pallas_call | solution.py:443
  63.2 7.0 %state.1 = (bf16[64,128]{1,0:T(8,128)(2,1)}, f32[8,4,256,512]{3,2,1,0:T(8,128)}) custom-call(f32[8,1024]{1,0:T(8,128)S(1)} %get-tuple-element.6.k_ref, f32[8,2048]{1,0:T(8,128)S(1)} %get-tuple-element.7.v_ref, bf16[64,128]{1,0:T(8,128)(2,1)S(1)} %get-tuple-element.8.act_ref, f32[4]{0:T(128)S(1)} %dynamic_slice.3.rate_ref, ...), custom_call_target="tpu_custom_call" | custom-call | flops 12582912 | bytes 33554432 | tf_op jit(solution)/shard_map/state/pallas_call | solution.py:498
  (1 shorter events, 0.0 us)

commit v3 on v2

--- a/solution.py
+++ b/solution.py
@@ -19,6 +19,10 @@
 WIDTH = 512
 LAG_A, LAG_B = 5, 5
 LAG_1, LAG_2, LAG_3, LAG_4 = 4, 4, 4, 3
+DIRECT_A, DIRECT_M, DIRECT_U, DIRECT_H = 3, 2, 3, 2
+HOLD, EARLY = 6, 2
+FIRST = 0
+CHUNKS = 1
 
 
 def head_decays(count):
@@ -71,12 +75,18 @@
     return finish
 
 
+def send_order(s, direct):
+    if s < FIRST:
+        return s + direct
+    return s - FIRST if s < FIRST + direct else s
+
+
 class PairScatter:
-    def __init__(self, kv, n_kv, rows, part, got, summed, got2, sends, sem_a, sem_b):
-        self.n_z = n_kv // PAIR
+    def __init__(self, kv, n_kv, rows, direct, bufs, sends, sem_a, sem_b):
+        self.kv, self.n_kv, self.n_z = kv, n_kv, n_kv // PAIR
         self.z, self.y = lax.div(kv, PAIR), lax.rem(kv, PAIR)
-        self.rows = rows
-        self.part, self.got, self.summed, self.got2 = part, got, summed, got2
+        self.rows, self.direct = rows, direct
+        self.part, self.got, self.summed, self.got2, self.got_all = bufs
         self.sends, self.sem_a, self.sem_b = sends, sem_a, sem_b
 
     def start(self, p, value):
@@ -85,6 +95,17 @@
             for y in range(PAIR):
                 at = (z * PAIR + y) * rows
                 self.part[p, y, z] = value[at : at + rows].astype(BF16)
+        if p < self.direct:
+            for d in range(1, self.n_kv):
+                peer = lax.rem(self.kv + d, self.n_kv)
+                put(
+                    self.part.at[p, lax.rem(peer, PAIR), lax.div(peer, PAIR)],
+                    self.got_all.at[p, d - 1],
+                    self.sends.at[2],
+                    self.sem_b.at[p],
+                    {"kv": peer},
+                )
+            return
         other = 1 - self.y
         put(
             self.part.at[p, other],
@@ -95,6 +116,8 @@
         )
 
     def middle(self, p):
+        if p < self.direct:
+            return
         landed(self.got.at[p], self.sem_a.at[p])
         self.summed[p] = (self.part[p, self.y].astype(F32) + self.got[p].astype(F32)).astype(BF16)
         for d in range(1, self.n_z):
@@ -108,30 +131,47 @@
             )
 
     def finish(self, p):
-        landed(self.got2.at[p], self.sem_b.at[p])
-        total = self.summed[p, self.z].astype(F32)
-        for d in range(self.n_z - 1):
-            total = total + self.got2[p, d].astype(F32)
+        if p < self.direct:
+            landed(self.got_all.at[p], self.sem_b.at[p])
+            own, got = self.part[p, self.y, self.z], self.got_all
+        else:
+            landed(self.got2.at[p], self.sem_b.at[p])
+            own, got = self.summed[p, self.z], self.got2
+        total = own.astype(F32)
+        for d in range(got.shape[1]):
+            total = total + got[p, d].astype(F32)
         return total
 
     def drain(self):
-        landed(self.got, self.sends.at[0])
-        landed(self.got2, self.sends.at[1])
+        rest = pl.ds(self.direct, self.got.shape[0] - self.direct)
+        landed(self.got.at[rest], self.sends.at[0])
+        landed(self.got2.at[rest], self.sends.at[1])
+        if self.direct:
+            landed(self.got_all.at[pl.ds(0, self.direct)], self.sends.at[2])
 
 
 class PairGather:
-    def __init__(self, kv, n_kv, buf, sends, sem_z, sem_y):
-        self.n_z = n_kv // PAIR
+    def __init__(self, kv, n_kv, direct, buf, like, sends, sem_z, sem_y):
+        self.kv, self.n_kv, self.n_z = kv, n_kv, n_kv // PAIR
         self.z, self.y = lax.div(kv, PAIR), lax.rem(kv, PAIR)
-        self.buf, self.sends, self.sem_z, self.sem_y = buf, sends, sem_z, sem_y
+        self.relayed, self.direct = buf.shape[0] - direct, direct
+        self.buf, self.like = buf, like
+        self.sends, self.sem_z, self.sem_y = sends, sem_z, sem_y
 
     def start(self, p):
         own = self.buf.at[p, self.z, self.y]
+        if p >= self.relayed:
+            for d in range(1, self.n_kv):
+                peer = {"kv": lax.rem(self.kv + d, self.n_kv)}
+                put(own, own, self.sends.at[2], self.sem_z.at[p], peer)
+            return
         for d in range(1, self.n_z):
             peer = lax.rem(self.z + d, self.n_z)
             put(own, own, self.sends.at[0], self.sem_z.at[p], {"kv": peer * PAIR + self.y})
 
     def relay(self, p):
+        if p >= self.relayed:
+            return
         landed(self.buf.at[p, pl.ds(0, self.n_z - 1), 0], self.sem_z.at[p])
         put(
             self.buf.at[p, :, self.y],
@@ -142,28 +182,34 @@
         )
 
     def finish(self, p):
-        landed(self.buf.at[p, :, 0], self.sem_y.at[p])
+        if p >= self.relayed:
+            landed(self.like.at[0], self.sem_z.at[p])
+        else:
+            landed(self.buf.at[p, :, 0], self.sem_y.at[p])
         blocks = [
             self.buf[p, z, y].astype(F32) for z in range(self.n_z) for y in range(PAIR)
         ]
         return jnp.concatenate(blocks, axis=0).astype(BF16)
 
     def drain(self):
-        landed(self.buf.at[:, pl.ds(0, self.n_z - 1), 0], self.sends.at[0])
-        landed(self.buf.at[:, :, 0], self.sends.at[1])
+        rest = pl.ds(0, self.relayed)
+        landed(self.buf.at[rest, pl.ds(0, self.n_z - 1), 0], self.sends.at[0])
+        landed(self.buf.at[rest, :, 0], self.sends.at[1])
+        if self.direct:
+            landed(self.like.at[pl.ds(0, self.direct)], self.sends.at[2])
 
 
 def fused_kernel(sizes, rate_ref, x_hbm, mg_hbm, cg_hbm, *refs):
     n_kv, n_tp, rows, width, dk, dv, heads, dim = sizes
     (qw_hbm, kw_hbm, vw_hbm, gw_hbm, ow_hbm, up_hbm, down_hbm, old_hbm) = refs[:8]
-    (out_ref, k_ref, v_ref, held) = refs[8:12]
-    (pack, gain_in, qw, kw, vw, gw, ow, up, down) = refs[12:21]
-    (part, got, summed, got2, part_u, got_u, summed_u, got2_u) = refs[21:29]
-    (sq_src, sq_dst, sq_src2, sq_dst2, mixes, hid, ret, acc) = refs[29:37]
-    (pair_own, pair_got, chip, far, mids, ends, got_ends) = refs[37:44]
-    (w_sem, s_sem, in_sem, t_sem, sq_sem, sq_sem2) = refs[44:50]
-    (sem_a, sem_b, sem_ua, sem_ub, mz_sem, my_sem, hz_sem, hy_sem) = refs[50:58]
-    (c_sem, far_sem, f_sem, s_send, u_send, m_send, h_send) = refs[58:65]
+    (out_ref, held) = refs[8:10]
+    (pack, gain_in, qw, kw, vw, gw, ow, up, down) = refs[10:19]
+    bufs, bufs_u, refs = refs[19:24], refs[24:29], refs[29:]
+    (sq_src, sq_dst, sq_src2, sq_dst2, mixes, hid, ret, acc, keys, vals) = refs[:10]
+    (pair_own, pair_got, chip, far, mids, ends, got_ends) = refs[10:17]
+    (w_sem, s_sem, in_sem, t_sem, sq_sem, sq_sem2) = refs[17:23]
+    (sems, sems_u, sems_m, sems_h) = refs[23:26], refs[26:29], refs[29:32], refs[32:35]
+    (c_sem, far_sem, f_sem) = refs[35:38]
     kv, tp = lax.axis_index("kv"), lax.axis_index("tp")
     z, y = lax.div(kv, PAIR), lax.rem(kv, PAIR)
     n_x = n_tp // CORES
@@ -214,14 +260,17 @@
     stream = [pack[t, :batch].astype(F32) for t in range(n_tp)]
     normed = normalise(stream, batch)
     sq_total = square_total(squares_of(stream), sq_src, sq_dst, kv, n_kv, rows, sq_sem)
-    scatter = PairScatter(kv, n_kv, rows, part, got, summed, got2, s_send, sem_a, sem_b)
-    mix_gather = PairGather(kv, n_kv, mixes, m_send, mz_sem, my_sem)
+    scatter = PairScatter(kv, n_kv, rows, DIRECT_A, bufs, *sems)
+    mix_gather = PairGather(kv, n_kv, DIRECT_M, mixes, bufs[4], *sems_m)
+
+    ready = set()
 
     def project(p):
         h, kind = divmod(p, 3)
-        if h == 0:
-            for name in (("q", "k"), ("v",), ("g",))[kind]:
+        for name in (("q", "k"), ("v",), ("g",))[kind]:
+            if name not in ready:
                 loads[name].wait()
+                ready.add(name)
         if kind == 0:
             cols = slice(h * dk, (h + 1) * dk)
             return jnp.concatenate(
@@ -247,6 +296,15 @@
         out = out * lax.rsqrt(jnp.mean(out * out, axis=1, keepdims=True) + EPS)
         mixes[h, z, y] = (jax.nn.silu(gate) * out).astype(BF16)
 
+    def update(h):
+        columns, value = keys[h].T, vals[h]
+        step = min(dk, 64)
+        for s in range(rows):
+            line = value[s : s + 1]
+            for r in range(0, dk, step):
+                term = columns[r : r + step, s : s + 1] * line
+                held[s, h, r : r + step] = rate_ref[h] * held[s, h, r : r + step] + term
+
     def attend(h):
         if h == 0:
             loads["ow"].wait()
@@ -256,10 +314,11 @@
         acc[...] = term if h == 0 else acc[...] + term
 
     pieces = 3 * heads
-    scale, values = None, {}
+    scale, values, pending = None, {}, []
     for s in range(pieces + LAG_A + LAG_B):
         if s < pieces:
-            scatter.start(s, project(s))
+            first = send_order(s, DIRECT_A)
+            scatter.start(first, project(first))
         if s == 0:
             load("ow", ow_hbm, ow, w_sem.at[4])
             load("up", up_hbm, up, w_sem.at[5])
@@ -275,23 +334,28 @@
             total = scatter.finish(p) * scale
             if kind == 0:
                 query, key = total[:, :dk], total[:, dk:] * dk ** (-0.5)
-                k_ref[:, h * dk : (h + 1) * dk] = key
+                keys[h] = key
                 values["q"], values["k"] = query, key
             elif kind == 1:
-                v_ref[:, h * dv : (h + 1) * dv] = total
+                vals[h] = total
                 values["v"] = total
             else:
                 if h == 0:
                     loads["old"].wait()
                 retain(h, values["q"], values["k"], values["v"], total)
-                mix_gather.start(h)
-                if h == heads - 1:
-                    for g in range(max(heads - 1, 0)):
-                        mix_gather.relay(g)
-                    for g in range(max(heads - 2, 0)):
-                        attend(g)
-    mix_gather.relay(heads - 1)
-    for h in range(max(heads - 2, 0), heads):
+                if h < heads - 1:
+                    pending.append(h)
+                else:
+                    mix_gather.start(h)
+            if p >= HOLD:
+                for g in pending:
+                    mix_gather.start(g)
+                pending = []
+    for h in range(heads - 1):
+        mix_gather.relay(h)
+    for h in range(min(EARLY, heads - 1)):
+        update(h)
+    for h in range(heads):
         attend(h)
 
     half = pair_own.shape[1] // 2
@@ -313,6 +377,8 @@
                 far_sem.at[1],
                 {"tp": peer},
             )
+    for h in range(min(EARLY, heads - 1), heads):
+        update(h)
     landed(far, far_sem.at[1])
     sums = []
     for j in range(CORES):
@@ -328,17 +394,16 @@
     stream = [mids[t].astype(F32) for t in range(n_tp)]
     normed_mid = normalise(stream, batch + GAIN_ROWS)
     sq_total2 = square_total(squares_of(stream), sq_src2, sq_dst2, kv, n_kv, rows, sq_sem2)
-    lift = PairScatter(
-        kv, n_kv, rows, part_u, got_u, summed_u, got2_u, u_send, sem_ua, sem_ub
-    )
-    gather = PairGather(kv, n_kv, hid, h_send, hz_sem, hy_sem)
+    lift = PairScatter(kv, n_kv, rows, DIRECT_U, bufs_u, *sems_u)
+    gather = PairGather(kv, n_kv, DIRECT_H, hid, bufs_u[4], *sems_h)
     count = up.shape[1] // width
     loads["up"].wait()
     scale2 = None
     for s in range(count + LAG_1 + LAG_2 + LAG_3 + LAG_4):
         if s < count:
-            w = up[:, s * width : (s + 1) * width]
-            lift.start(s, jnp.dot(normed_mid, w, preferred_element_type=F32))
+            first = send_order(s, DIRECT_U)
+            w = up[:, first * width : (first + 1) * width]
+            lift.start(first, jnp.dot(normed_mid, w, preferred_element_type=F32))
         p = s - LAG_1
         if 0 <= p < count:
             lift.middle(p)
@@ -377,36 +442,19 @@
     landed(got_ends, f_sem.at[0])
 
 
-def state_kernel(heads, dk, dv, k_ref, v_ref, act_ref, rate_ref, old_ref, *refs):
-    act_out, out_ref, new_ref, sem, act_sem = refs
-    step = min(dk, 64)
-    seqs = k_ref.shape[0]
-    act_copy = pltpu.make_async_copy(act_ref, act_out, act_sem)
-    act_copy.start()
-
-    def write(s, h):
-        return pltpu.make_async_copy(new_ref.at[s, h], out_ref.at[s, h], sem.at[s, h])
-
-    def one(s, carry):
-        k_row = k_ref[pl.ds(s, 1), :]
-        lines = [k_row[:, h * dk : (h + 1) * dk] for h in range(heads)]
-        lines.append(jnp.zeros((-heads % 8, dk), F32))
-        columns = jnp.concatenate(lines, axis=0).T
-        for h in range(heads):
-            value = v_ref[pl.ds(s, 1), h * dv : (h + 1) * dv]
-            for r in range(0, dk, step):
-                key = columns[r : r + step, h : h + 1]
-                new_ref[s, h, r : r + step] = (
-                    rate_ref[h] * old_ref[s, h, r : r + step] + key * value
-                )
-            write(s, h).start()
-        return carry
-
-    lax.fori_loop(0, seqs, one, 0, unroll=2)
-    for s in range(seqs):
-        for h in range(heads):
-            write(s, h).wait()
-    act_copy.wait()
+def write_kernel(act_ref, state_ref, act_out, state_out, act_sem, sem):
+    copies = [pltpu.make_async_copy(act_ref, act_out, act_sem)]
+    for s in range(state_ref.shape[0]):
+        for h in range(CHUNKS):
+            n = state_ref.shape[1] // CHUNKS
+            part = (s, pl.ds(h * n, n))
+            copies.append(
+                pltpu.make_async_copy(state_ref.at[part], state_out.at[part], sem.at[s, h])
+            )
+    for copy in copies:
+        copy.start()
+    for copy in copies:
+        copy.wait()
 
 
 def in_hbm(a):
@@ -418,13 +466,14 @@
 ANY = pl.BlockSpec(memory_space=pltpu.HBM)
 
 
-def scatter_scratch(count, n_kv, rows, width):
+def scatter_scratch(count, n_kv, rows, width, direct):
     n_z = n_kv // PAIR
     return [
         pltpu.VMEM((count, PAIR, n_z, rows, width), BF16),
         pltpu.VMEM((count, n_z, rows, width), BF16),
         pltpu.VMEM((count, n_z, rows, width), BF16),
         pltpu.VMEM((count, n_z - 1, rows, width), BF16),
+        pltpu.VMEM((max(direct, 1), n_kv - 1, rows, width), BF16),
     ]
 
 
@@ -440,22 +489,20 @@
         head_decays(HEADS), lax.axis_index("tp") * heads, heads, 0
     )
     elements = sum(w.size for w in (qw, kw, vw, gw, ow, uw, dw))
-    out, key, value, held = pl.pallas_call(
+    out, held = pl.pallas_call(
         functools.partial(fused_kernel, (n_kv, n_tp, seqs, width, dk, dv, heads, dim)),
         out_shape=[
             jax.ShapeDtypeStruct((batch, block), BF16),
-            jax.ShapeDtypeStruct((seqs, heads * dk), F32),
-            jax.ShapeDtypeStruct((seqs, heads * dv), F32),
             pltpu.VMEM(state.shape, F32),
         ],
         in_specs=[SM] + [ANY] * 11,
-        out_specs=[VM] * 4,
+        out_specs=[VM] * 2,
         scratch_shapes=[
             pltpu.VMEM((n_tp, batch + 2 * GAIN_ROWS, block), BF16),
             pltpu.VMEM((2, 1, block), BF16),
             *[pltpu.VMEM(w.shape, BF16) for w in (qw, kw, vw, gw, ow, uw, dw)],
-            *scatter_scratch(pieces, n_kv, seqs, dv),
-            *scatter_scratch(count, n_kv, seqs, width),
+            *scatter_scratch(pieces, n_kv, seqs, dv, max(DIRECT_A, DIRECT_M)),
+            *scatter_scratch(count, n_kv, seqs, width, max(DIRECT_U, DIRECT_H)),
             pltpu.VMEM((n_kv, seqs, 128), F32),
             pltpu.VMEM((n_kv - 1, seqs, 128), F32),
             pltpu.VMEM((n_kv, seqs, 128), F32),
@@ -464,6 +511,8 @@
             pltpu.VMEM((count, n_z, PAIR, seqs, width), BF16),
             pltpu.VMEM((seqs, dv), F32),
             pltpu.VMEM((batch, cols), F32),
+            pltpu.VMEM((heads, seqs, dk), F32),
+            pltpu.VMEM((heads, seqs, dv), F32),
             pltpu.VMEM((batch, cols), BF16),
             pltpu.VMEM((batch, cols), BF16),
             pltpu.VMEM((CORES, batch, cols // CORES), BF16),
@@ -475,11 +524,11 @@
             DMA,
             DMA((3,)),
             *[DMA((2,))] * 3,
-            *[DMA((pieces,))] * 2,
-            *[DMA((count,))] * 2,
-            *[DMA((heads,))] * 2,
-            *[DMA((count,))] * 2,
-            *[DMA((2,))] * 7,
+            *[DMA((3,)), *[DMA((pieces,))] * 2],
+            *[DMA((3,)), *[DMA((count,))] * 2],
+            *[DMA((3,)), *[DMA((heads,))] * 2],
+            *[DMA((3,)), *[DMA((count,))] * 2],
+            *[DMA((2,))] * 3,
         ],
         compiler_params=pltpu.CompilerParams(
             collective_id=0, has_side_effects=True, vmem_limit_bytes=26 * 2**20
@@ -496,17 +545,17 @@
         *[in_hbm(a) for a in (qw, kw, vw, gw, ow, uw, dw, state)],
     )
     return pl.pallas_call(
-        functools.partial(state_kernel, heads, dk, dv),
+        write_kernel,
         out_shape=[pltpu.HBM((batch, block), BF16), pltpu.HBM(state.shape, F32)],
-        in_specs=[VM, VM, VM, SM, VM],
+        in_specs=[VM, VM],
         out_specs=[ANY, ANY],
-        scratch_shapes=[pltpu.VMEM(state.shape, F32), DMA((seqs, heads)), DMA],
-        compiler_params=pltpu.CompilerParams(vmem_limit_bytes=18 * 2**20),
+        scratch_shapes=[DMA, DMA((seqs, CHUNKS))],
+        compiler_params=pltpu.CompilerParams(vmem_limit_bytes=2**20),
         cost_estimate=pl.CostEstimate(
-            flops=3 * state.size, bytes_accessed=8 * state.size, transcendentals=0
+            flops=state.size, bytes_accessed=4 * state.size, transcendentals=0
         ),
-        name="state",
-    )(key, value, out, rates, held)
+        name="write",
+    )(out, held)
 
 
 def solution(mesh):

time: 70.5 us -> 63.9 us (0.906)
  Pallas kernels: 69.5 us -> 62.9 us
    pallas_call x1, Pallas kernels: 62.5 us -> 57 us  [fused_device(): pl.pallas_call(functools.partial(fused_kernel, (n_kv, n_tp, seqs, width,...]
    pallas_call x1, Pallas kernels: 6.97 us -> 5.94 us  [fused_device(): pl.pallas_call(write_kernel, out_shape=[pltpu.HBM((batch, block), BF16),...]
where the time goes in v3:
time: 63.9 us; the launch traced here: 63.7 us
  Pallas kernels  62.9 us (98%)
  between operations  0.65 us (1%)
    pallas_call x1, Pallas kernels, fused_device(): pl.pallas_call(functools.partial(fused_kernel, (n_kv, n_tp, seqs, width,...  57 us
    pallas_call x1, Pallas kernels, fused_device(): pl.pallas_call(write_kernel, out_shape=[pltpu.HBM((batch, block), BF16),...  5.94 us

profile of v3, /device:TPU:0, one launch (start us, length us, event | category | flops | bytes accessed | tf_op | source)
XLA Modules:
  0.0 63.7 jit_solution(10701950926278100719)
XLA Ops:
  0.6 0.1 dynamic_slice.3.rate_ref
  0.7 57.0 %fused.1 = (bf16[64,128]{1,0:T(8,128)(2,1)S(1)}, f32[8,4,256,512]{3,2,1,0:T(8,128)S(1)}) custom-call(f32[4]{0:T(128)S(1)} %dynamic_slice.3.rate_ref, bf16[64,128]{1,0:T(8,128)(2,1)} %x_hbm.1, bf16[1,128]{1,0:T(2,128)(2,1)} %bitcast.2, bf16[1,128]{1,0:T(2,128)(2,1)} %bitcast.3, bf16[512,1024]{1,0:T(8,128)(2,1)} %refs_0_.1, bf16[512,1024]{1,0:T(8,128)(2,1)} %refs_1_.1, ...), custom_call_target="tpu_custom_call" | custom-call | flops 1073741824 | bytes 33554432 | tf_op jit(solution)/shard_map/fused/pallas_call | solution.py:492
  57.7 5.9 %write.1 = (bf16[64,128]{1,0:T(8,128)(2,1)}, f32[8,4,256,512]{3,2,1,0:T(8,128)}) custom-call(bf16[64,128]{1,0:T(8,128)(2,1)S(1)} %get-tuple-element.4.act_ref, f32[8,4,256,512]{3,2,1,0:T(8,128)S(1)} %get-tuple-element.5.state_ref), custom_call_target="tpu_custom_call" | custom-call | flops 4194304 | bytes 16777216 | tf_op jit(solution)/shard_map/write/pallas_call | solution.py:547
  (1 shorter events, 0.0 us)

commit v4 on v3

--- a/solution.py
+++ b/solution.py
@@ -283,7 +283,7 @@
         w = (vw, gw)[kind - 1]
         return jnp.dot(normed, w[:, h * dv : (h + 1) * dv], preferred_element_type=F32)
 
-    def retain(h, query, key, value, gate):
+    def retain(h, query, key, value):
         columns = query.T
         step = min(dk, 64)
         for s in range(rows):
@@ -293,8 +293,7 @@
                 total = total + jnp.sum(term.reshape(step // 8, 8, dv), axis=0)
             ret[s : s + 1] = jnp.sum(total, axis=0, keepdims=True)
         out = rate_ref[h] * ret[...] + jnp.sum(query * key, axis=1, keepdims=True) * value
-        out = out * lax.rsqrt(jnp.mean(out * out, axis=1, keepdims=True) + EPS)
-        mixes[h, z, y] = (jax.nn.silu(gate) * out).astype(BF16)
+        ret[...] = out * lax.rsqrt(jnp.mean(out * out, axis=1, keepdims=True) + EPS)
 
     def update(h):
         columns, value = keys[h].T, vals[h]
@@ -338,11 +337,11 @@
                 values["q"], values["k"] = query, key
             elif kind == 1:
                 vals[h] = total
-                values["v"] = total
-            else:
                 if h == 0:
                     loads["old"].wait()
-                retain(h, values["q"], values["k"], values["v"], total)
+                retain(h, values["q"], values["k"], total)
+            else:
+                mixes[h, z, y] = (jax.nn.silu(total) * ret[...]).astype(BF16)
                 if h < heads - 1:
                     pending.append(h)
                 else:

time: 63.9 us -> 63.3 us (level)
    pallas_call x1, Pallas kernels: 57 us -> 56.3 us  [fused_device(): pl.pallas_call(functools.partial(fused_kernel, (n_kv, n_tp, seqs, width,...]
where the time goes in v4:
time: 63.3 us; the launch traced here: 63 us
  Pallas kernels  62.3 us (98%)
  between operations  0.65 us (1%)
    pallas_call x1, Pallas kernels, fused_device(): pl.pallas_call(functools.partial(fused_kernel, (n_kv, n_tp, seqs, width,...  56.3 us
    pallas_call x1, Pallas kernels, fused_device(): pl.pallas_call(write_kernel, out_shape=[pltpu.HBM((batch, block), BF16),...  5.94 us

profile of v4, /device:TPU:0, one launch (start us, length us, event | category | flops | bytes accessed | tf_op | source)
XLA Modules:
  0.0 63.0 jit_solution(6667734226661772242)
XLA Ops:
  0.6 0.1 dynamic_slice.3.rate_ref
  0.7 56.3 %fused.1 = (bf16[64,128]{1,0:T(8,128)(2,1)S(1)}, f32[8,4,256,512]{3,2,1,0:T(8,128)S(1)}) custom-call(f32[4]{0:T(128)S(1)} %dynamic_slice.3.rate_ref, bf16[64,128]{1,0:T(8,128)(2,1)} %x_hbm.1, bf16[1,128]{1,0:T(2,128)(2,1)} %bitcast.2, bf16[1,128]{1,0:T(2,128)(2,1)} %bitcast.3, bf16[512,1024]{1,0:T(8,128)(2,1)} %refs_0_.1, bf16[512,1024]{1,0:T(8,128)(2,1)} %refs_1_.1, ...), custom_call_target="tpu_custom_call" | custom-call | flops 1073741824 | bytes 33554432 | tf_op jit(solution)/shard_map/fused/pallas_call | solution.py:491
  57.1 5.9 %write.1 = (bf16[64,128]{1,0:T(8,128)(2,1)}, f32[8,4,256,512]{3,2,1,0:T(8,128)}) custom-call(bf16[64,128]{1,0:T(8,128)(2,1)S(1)} %get-tuple-element.4.act_ref, f32[8,4,256,512]{3,2,1,0:T(8,128)S(1)} %get-tuple-element.5.state_ref), custom_call_target="tpu_custom_call" | custom-call | flops 4194304 | bytes 16777216 | tf_op jit(solution)/shard_map/write/pallas_call | solution.py:546
  (1 shorter events, 0.0 us)

commit v5 on v4

--- a/solution.py
+++ b/solution.py
@@ -19,9 +19,11 @@
 WIDTH = 512
 LAG_A, LAG_B = 5, 5
 LAG_1, LAG_2, LAG_3, LAG_4 = 4, 4, 4, 3
-DIRECT_A, DIRECT_M, DIRECT_U, DIRECT_H = 3, 2, 3, 2
+DIRECT_M, DIRECT_H = 2, 2
+ALONG_A, ALONG_U = (3, 4), (3, 4)
+SEND = (0, 3, 4, 1, 2)
+FOLD = (0, 1, 2, 3, 5, 4)
 HOLD, EARLY = 6, 2
-FIRST = 0
 CHUNKS = 1
 
 
@@ -75,18 +77,17 @@
     return finish
 
 
-def send_order(s, direct):
-    if s < FIRST:
-        return s + direct
-    return s - FIRST if s < FIRST + direct else s
+def in_order(order, s):
+    return order[s] if s < len(order) else s
 
 
 class PairScatter:
-    def __init__(self, kv, n_kv, rows, direct, bufs, sends, sem_a, sem_b):
+    def __init__(self, kv, n_kv, rows, along, bufs, sends, sem_a, sem_b):
         self.kv, self.n_kv, self.n_z = kv, n_kv, n_kv // PAIR
         self.z, self.y = lax.div(kv, PAIR), lax.rem(kv, PAIR)
-        self.rows, self.direct = rows, direct
-        self.part, self.got, self.summed, self.got2, self.got_all = bufs
+        self.rows, self.other = rows, {"kv": self.z * PAIR + 1 - self.y}
+        self.part, self.got, self.summed, self.got2, self.got_all, self.kept = bufs
+        self.along = {p: i for i, p in enumerate(along) if p < self.got.shape[0]}
         self.sends, self.sem_a, self.sem_b = sends, sem_a, sem_b
 
     def start(self, p, value):
@@ -95,28 +96,45 @@
             for y in range(PAIR):
                 at = (z * PAIR + y) * rows
                 self.part[p, y, z] = value[at : at + rows].astype(BF16)
-        if p < self.direct:
-            for d in range(1, self.n_kv):
-                peer = lax.rem(self.kv + d, self.n_kv)
+        if p in self.along:
+            for d in range(1, self.n_z):
+                peer = lax.rem(self.z + d, self.n_z)
                 put(
-                    self.part.at[p, lax.rem(peer, PAIR), lax.div(peer, PAIR)],
-                    self.got_all.at[p, d - 1],
+                    self.part.at[p, :, peer],
+                    self.got_all.at[self.along[p], pl.ds((d - 1) * PAIR, PAIR)],
                     self.sends.at[2],
                     self.sem_b.at[p],
-                    {"kv": peer},
+                    {"kv": peer * PAIR + self.y},
                 )
             return
-        other = 1 - self.y
         put(
-            self.part.at[p, other],
+            self.part.at[p, 1 - self.y],
             self.got.at[p],
             self.sends.at[0],
             self.sem_a.at[p],
-            {"kv": self.z * PAIR + other},
+            self.other,
         )
 
     def middle(self, p):
-        if p < self.direct:
+        if p in self.along:
+            at, count = self.along[p], (self.n_z - 1) * PAIR
+            landed(self.got_all.at[at, pl.ds(0, count)], self.sem_b.at[p])
+
+            def total(y):
+                value = self.part[p, y, self.z].astype(F32)
+                for d in range(0, count, PAIR):
+                    value = value + self.got_all[at, d + y].astype(F32)
+                return value
+
+            self.summed[p, 0] = total(1 - self.y).astype(BF16)
+            self.kept[at] = total(self.y)
+            put(
+                self.summed.at[p, 0],
+                self.got.at[p, 0],
+                self.sends.at[3],
+                self.sem_a.at[p],
+                self.other,
+            )
             return
         landed(self.got.at[p], self.sem_a.at[p])
         self.summed[p] = (self.part[p, self.y].astype(F32) + self.got[p].astype(F32)).astype(BF16)
@@ -131,23 +149,24 @@
             )
 
     def finish(self, p):
-        if p < self.direct:
-            landed(self.got_all.at[p], self.sem_b.at[p])
-            own, got = self.part[p, self.y, self.z], self.got_all
-        else:
-            landed(self.got2.at[p], self.sem_b.at[p])
-            own, got = self.summed[p, self.z], self.got2
-        total = own.astype(F32)
-        for d in range(got.shape[1]):
-            total = total + got[p, d].astype(F32)
+        if p in self.along:
+            landed(self.got.at[p, 0], self.sem_a.at[p])
+            return self.kept[self.along[p]] + self.got[p, 0].astype(F32)
+        landed(self.got2.at[p], self.sem_b.at[p])
+        total = self.summed[p, self.z].astype(F32)
+        for d in range(self.n_z - 1):
+            total = total + self.got2[p, d].astype(F32)
         return total
 
     def drain(self):
-        rest = pl.ds(self.direct, self.got.shape[0] - self.direct)
+        n = len(self.along)
+        rest = pl.ds(0, self.got.shape[0] - n)
         landed(self.got.at[rest], self.sends.at[0])
         landed(self.got2.at[rest], self.sends.at[1])
-        if self.direct:
-            landed(self.got_all.at[pl.ds(0, self.direct)], self.sends.at[2])
+        if n:
+            blocks = self.got_all.at[pl.ds(0, n), pl.ds(0, (self.n_z - 1) * PAIR)]
+            landed(blocks, self.sends.at[2])
+            landed(self.got.at[pl.ds(0, n), 0], self.sends.at[3])
 
 
 class PairGather:
@@ -204,7 +223,7 @@
     (qw_hbm, kw_hbm, vw_hbm, gw_hbm, ow_hbm, up_hbm, down_hbm, old_hbm) = refs[:8]
     (out_ref, held) = refs[8:10]
     (pack, gain_in, qw, kw, vw, gw, ow, up, down) = refs[10:19]
-    bufs, bufs_u, refs = refs[19:24], refs[24:29], refs[29:]
+    bufs, bufs_u, refs = refs[19:25], refs[25:31], refs[31:]
     (sq_src, sq_dst, sq_src2, sq_dst2, mixes, hid, ret, acc, keys, vals) = refs[:10]
     (pair_own, pair_got, chip, far, mids, ends, got_ends) = refs[10:17]
     (w_sem, s_sem, in_sem, t_sem, sq_sem, sq_sem2) = refs[17:23]
@@ -260,7 +279,7 @@
     stream = [pack[t, :batch].astype(F32) for t in range(n_tp)]
     normed = normalise(stream, batch)
     sq_total = square_total(squares_of(stream), sq_src, sq_dst, kv, n_kv, rows, sq_sem)
-    scatter = PairScatter(kv, n_kv, rows, DIRECT_A, bufs, *sems)
+    scatter = PairScatter(kv, n_kv, rows, ALONG_A, bufs, *sems)
     mix_gather = PairGather(kv, n_kv, DIRECT_M, mixes, bufs[4], *sems_m)
 
     ready = set()
@@ -316,7 +335,7 @@
     scale, values, pending = None, {}, []
     for s in range(pieces + LAG_A + LAG_B):
         if s < pieces:
-            first = send_order(s, DIRECT_A)
+            first = in_order(SEND, s)
             scatter.start(first, project(first))
         if s == 0:
             load("ow", ow_hbm, ow, w_sem.at[4])
@@ -324,7 +343,7 @@
             load("down", down_hbm, down, w_sem.at[6])
         p = s - LAG_A
         if 0 <= p < pieces:
-            scatter.middle(p)
+            scatter.middle(in_order(FOLD, p))
         p = p - LAG_B
         if 0 <= p < pieces:
             if p == 0:
@@ -393,19 +412,19 @@
     stream = [mids[t].astype(F32) for t in range(n_tp)]
     normed_mid = normalise(stream, batch + GAIN_ROWS)
     sq_total2 = square_total(squares_of(stream), sq_src2, sq_dst2, kv, n_kv, rows, sq_sem2)
-    lift = PairScatter(kv, n_kv, rows, DIRECT_U, bufs_u, *sems_u)
+    lift = PairScatter(kv, n_kv, rows, ALONG_U, bufs_u, *sems_u)
     gather = PairGather(kv, n_kv, DIRECT_H, hid, bufs_u[4], *sems_h)
     count = up.shape[1] // width
     loads["up"].wait()
     scale2 = None
     for s in range(count + LAG_1 + LAG_2 + LAG_3 + LAG_4):
         if s < count:
-            first = send_order(s, DIRECT_U)
+            first = in_order(SEND if count > 5 else (), s)
             w = up[:, first * width : (first + 1) * width]
             lift.start(first, jnp.dot(normed_mid, w, preferred_element_type=F32))
         p = s - LAG_1
         if 0 <= p < count:
-            lift.middle(p)
+            lift.middle(in_order(FOLD if count > 5 else (), p))
         p = p - LAG_2
         if 0 <= p < count:
             if p == 0:
@@ -473,6 +492,7 @@
         pltpu.VMEM((count, n_z, rows, width), BF16),
         pltpu.VMEM((count, n_z - 1, rows, width), BF16),
         pltpu.VMEM((max(direct, 1), n_kv - 1, rows, width), BF16),
+        pltpu.VMEM((max(direct, 1), rows, width), F32),
     ]
 
 
@@ -500,8 +520,8 @@
             pltpu.VMEM((n_tp, batch + 2 * GAIN_ROWS, block), BF16),
             pltpu.VMEM((2, 1, block), BF16),
             *[pltpu.VMEM(w.shape, BF16) for w in (qw, kw, vw, gw, ow, uw, dw)],
-            *scatter_scratch(pieces, n_kv, seqs, dv, max(DIRECT_A, DIRECT_M)),
-            *scatter_scratch(count, n_kv, seqs, width, max(DIRECT_U, DIRECT_H)),
+            *scatter_scratch(pieces, n_kv, seqs, dv, max(len(ALONG_A), DIRECT_M)),
+            *scatter_scratch(count, n_kv, seqs, width, max(len(ALONG_U), DIRECT_H)),
             pltpu.VMEM((n_kv, seqs, 128), F32),
             pltpu.VMEM((n_kv - 1, seqs, 128), F32),
             pltpu.VMEM((n_kv, seqs, 128), F32),
@@ -523,8 +543,8 @@
             DMA,
             DMA((3,)),
             *[DMA((2,))] * 3,
-            *[DMA((3,)), *[DMA((pieces,))] * 2],
-            *[DMA((3,)), *[DMA((count,))] * 2],
+            *[DMA((4,)), *[DMA((pieces,))] * 2],
+            *[DMA((4,)), *[DMA((count,))] * 2],
             *[DMA((3,)), *[DMA((heads,))] * 2],
             *[DMA((3,)), *[DMA((count,))] * 2],
             *[DMA((2,))] * 3,

time: 63.3 us -> 62.9 us (level)
  no operation moved by 1% of the time
where the time goes in v5:
time: 62.9 us; the launch traced here: 62.6 us
  Pallas kernels  61.9 us (98%)
  between operations  0.65 us (1%)
    pallas_call x1, Pallas kernels, fused_device(): pl.pallas_call(functools.partial(fused_kernel, (n_kv, n_tp, seqs, width,...  55.9 us
    pallas_call x1, Pallas kernels, fused_device(): pl.pallas_call(write_kernel, out_shape=[pltpu.HBM((batch, block), BF16),...  5.94 us

profile of v5, /device:TPU:0, one launch (start us, length us, event | category | flops | bytes accessed | tf_op | source)
XLA Modules:
  0.0 62.6 jit_solution(11562298581350257955)
XLA Ops:
  0.6 0.1 dynamic_slice.3.rate_ref
  0.7 55.9 %fused.1 = (bf16[64,128]{1,0:T(8,128)(2,1)S(1)}, f32[8,4,256,512]{3,2,1,0:T(8,128)S(1)}) custom-call(f32[4]{0:T(128)S(1)} %dynamic_slice.3.rate_ref, bf16[64,128]{1,0:T(8,128)(2,1)} %x_hbm.1, bf16[1,128]{1,0:T(2,128)(2,1)} %bitcast.2, bf16[1,128]{1,0:T(2,128)(2,1)} %bitcast.3, bf16[512,1024]{1,0:T(8,128)(2,1)} %refs_0_.1, bf16[512,1024]{1,0:T(8,128)(2,1)} %refs_1_.1, ...), custom_call_target="tpu_custom_call" | custom-call | flops 1073741824 | bytes 33554432 | tf_op jit(solution)/shard_map/fused/pallas_call | solution.py:511
  56.7 5.9 %write.1 = (bf16[64,128]{1,0:T(8,128)(2,1)}, f32[8,4,256,512]{3,2,1,0:T(8,128)}) custom-call(bf16[64,128]{1,0:T(8,128)(2,1)S(1)} %get-tuple-element.4.act_ref, f32[8,4,256,512]{3,2,1,0:T(8,128)S(1)} %get-tuple-element.5.state_ref), custom_call_target="tpu_custom_call" | custom-call | flops 4194304 | bytes 16777216 | tf_op jit(solution)/shard_map/write/pallas_call | solution.py:566
  (1 shorter events, 0.0 us)

commit v6 on v5

--- a/solution.py
+++ b/solution.py
@@ -227,8 +227,9 @@
     (sq_src, sq_dst, sq_src2, sq_dst2, mixes, hid, ret, acc, keys, vals) = refs[:10]
     (pair_own, pair_got, chip, far, mids, ends, got_ends) = refs[10:17]
     (w_sem, s_sem, in_sem, t_sem, sq_sem, sq_sem2) = refs[17:23]
-    (sems, sems_u, sems_m, sems_h) = refs[23:26], refs[26:29], refs[29:32], refs[32:35]
-    (c_sem, far_sem, f_sem) = refs[35:38]
+    sems, sems_h = refs[23:26], refs[28:31]
+    sems_u, sems_m = (refs[26], *sems[1:]), (refs[27], *sems_h[1:])
+    (c_sem, far_sem, f_sem) = refs[31:34]
     kv, tp = lax.axis_index("kv"), lax.axis_index("tp")
     z, y = lax.div(kv, PAIR), lax.rem(kv, PAIR)
     n_x = n_tp // CORES
@@ -543,10 +544,10 @@
             DMA,
             DMA((3,)),
             *[DMA((2,))] * 3,
-            *[DMA((4,)), *[DMA((pieces,))] * 2],
-            *[DMA((4,)), *[DMA((count,))] * 2],
-            *[DMA((3,)), *[DMA((heads,))] * 2],
-            *[DMA((3,)), *[DMA((count,))] * 2],
+            *[DMA((4,)), *[DMA((max(pieces, count),))] * 2],
+            DMA((4,)),
+            DMA((3,)),
+            *[DMA((3,)), *[DMA((max(heads, count),))] * 2],
             *[DMA((2,))] * 3,
         ],
         compiler_params=pltpu.CompilerParams(

time: 62.9 us -> 62.7 us (level)
  no operation moved by 1% of the time
where the time goes in v6:
time: 62.7 us; the launch traced here: 62.4 us
  Pallas kernels  61.7 us (98%)
  between operations  0.65 us (1%)
    pallas_call x1, Pallas kernels, fused_device(): pl.pallas_call(functools.partial(fused_kernel, (n_kv, n_tp, seqs, width,...  55.7 us
    pallas_call x1, Pallas kernels, fused_device(): pl.pallas_call(write_kernel, out_shape=[pltpu.HBM((batch, block), BF16),...  5.94 us

profile of v6, /device:TPU:0, one launch (start us, length us, event | category | flops | bytes accessed | tf_op | source)
XLA Modules:
  0.0 62.4 jit_solution(7656205440571063944)
XLA Ops:
  0.6 0.1 dynamic_slice.3.rate_ref
  0.7 55.7 %fused.1 = (bf16[64,128]{1,0:T(8,128)(2,1)S(1)}, f32[8,4,256,512]{3,2,1,0:T(8,128)S(1)}) custom-call(f32[4]{0:T(128)S(1)} %dynamic_slice.3.rate_ref, bf16[64,128]{1,0:T(8,128)(2,1)} %x_hbm.1, bf16[1,128]{1,0:T(2,128)(2,1)} %bitcast.2, bf16[1,128]{1,0:T(2,128)(2,1)} %bitcast.3, bf16[512,1024]{1,0:T(8,128)(2,1)} %refs_0_.1, bf16[512,1024]{1,0:T(8,128)(2,1)} %refs_1_.1, ...), custom_call_target="tpu_custom_call" | custom-call | flops 1073741824 | bytes 33554432 | tf_op jit(solution)/shard_map/fused/pallas_call | solution.py:512
  56.5 5.9 %write.1 = (bf16[64,128]{1,0:T(8,128)(2,1)}, f32[8,4,256,512]{3,2,1,0:T(8,128)}) custom-call(bf16[64,128]{1,0:T(8,128)(2,1)S(1)} %get-tuple-element.4.act_ref, f32[8,4,256,512]{3,2,1,0:T(8,128)S(1)} %get-tuple-element.5.state_ref), custom_call_target="tpu_custom_call" | custom-call | flops 4194304 | bytes 16777216 | tf_op jit(solution)/shard_map/write/pallas_call | solution.py:567
  (1 shorter events, 0.0 us)
